TPU v7x, 32 devices: a whole 2x2x4 slice. The times are simulated.
32 devices in a mesh: grp: 2 (over y), sp: 8 (over z, core), tp: 2 (over x).
Axes of the slice: x: 2, y: 2, z: 4, core: 2. Of those that a mesh axis runs over, the one named last changes fastest.
Arguments:
- queries: bfloat16 [12288, 1024], P(('grp', 'sp'), 'tp'), parts along dimension 0, may hold values from -200 to 200
- key_rows: bfloat16 [12288, 512], P(('grp', 'sp'), 'tp'), parts along dimension 0, may hold values from -6 to 6
- value_rows: bfloat16 [12288, 512], P(('grp', 'sp'), 'tp'), parts along dimension 0, may hold values from -6 to 6
- doc_ids: int32 [12288], P(('grp', 'sp')), parts along dimension 0, may hold values from 0 to 3, never falling along the last dimension, each value on 1 to 3072 neighbouring positions
- sink_logits: float32 [16], P('tp'), may hold values from 2 to 7
- out_weight: bfloat16 [1024, 2048], P('tp', 'sp'), may hold values from -0.1875 to 0.1875
- residual: bfloat16 [12288, 2048], P(('grp', 'sp', 'tp')), parts along dimension 0, may hold values from -6 to 6
- gain_mixed: float32 [2048], replicated, may hold values from 0.1 to 1.9
- gain_before: float32 [2048], replicated, may hold values from 0.1 to 1.9
- gain_after: float32 [2048], replicated, may hold values from 0.1 to 1.9
- gate_weight: bfloat16 [2048, 6144], P('sp', 'tp'), may hold values from -0.125 to 0.125
- up_weight: bfloat16 [2048, 6144], P('sp', 'tp'), may hold values from -0.125 to 0.125
- down_weight: bfloat16 [6144, 2048], P('tp', 'sp'), may hold values from -0.078125 to 0.078125
Outputs:
- layer_out: bfloat16 [12288, 2048], P(('grp', 'sp', 'tp')), parts along dimension 0
There are 2 independent parts, one for each index of `grp`. A program takes and returns all parts, laid end to end along the dimension named above; an argument that names none is the same for every part. Nothing has to cross between parts.
All inputs are finite; a program needn't handle non-finite values.
Results may differ from a plain program's by a relative error of at most 0.015.
Values may be sent and summed in bfloat16 or wider, within the bound.
A program may use at most 128 MiB of HBM per device.

v0:
```python
import functools

import jax
import jax.numpy as jnp
from jax import lax
from jax.experimental import pallas as pl
from jax.experimental.pallas import tpu as pltpu
from jax.sharding import PartitionSpec as P

HEAD_DIM = 64
WINDOW = 128


epsilon = 1e-06
masked_value = -1e30


def passed_along(value, axis, steps):
    count = lax.axis_size(axis)
    first, last = (max(0, -steps), min(count, count - steps))
    return lax.ppermute(value, axis, [(source, source + steps) for source in range(first, last)])


def stored(value):
    return lax.optimization_barrier(value.astype(jnp.bfloat16)).astype(jnp.float32)


def rms_scaled(value, gain):
    return value * lax.rsqrt(jnp.mean(value * value, axis=-1, keepdims=True) + epsilon) * gain


def windows(array, blocks):
    first = array[:-WINDOW].reshape((blocks, WINDOW) + array.shape[1:])
    second = array[WINDOW:].reshape((blocks, WINDOW) + array.shape[1:])
    return jnp.concatenate([first, second], axis=1)


def attend(queries, key_rows, value_rows, doc_ids, sink_logits):
    length = queries.shape[0]
    blocks = length // WINDOW
    local_kv = key_rows.shape[1] // HEAD_DIM
    group_size = queries.shape[1] // HEAD_DIM // local_kv
    offset = lax.axis_index("sp") * length
    tail_keys, tail_values, tail_docs = passed_along(
        (key_rows[length - WINDOW :], value_rows[length - WINDOW :], doc_ids[length - WINDOW :]),
        "sp",
        1,
    )
    key_blocks = windows(jnp.concatenate([tail_keys, key_rows], axis=0), blocks).reshape(
        blocks, 2 * WINDOW, local_kv, HEAD_DIM
    )
    value_blocks = windows(jnp.concatenate([tail_values, value_rows], axis=0), blocks).reshape(
        blocks, 2 * WINDOW, local_kv, HEAD_DIM
    )
    key_docs = windows(jnp.concatenate([tail_docs, doc_ids], axis=0), blocks)
    key_places = windows(offset - WINDOW + jnp.arange(length + WINDOW, dtype=jnp.int32), blocks)
    query_places = (offset + jnp.arange(length, dtype=jnp.int32)).reshape(blocks, WINDOW)
    query_docs = doc_ids.reshape(blocks, WINDOW)
    query_blocks = queries.reshape(blocks, WINDOW, local_kv, group_size, HEAD_DIM)
    scores = jnp.einsum(
        "bqhgd,bkhd->bhgqk", query_blocks, key_blocks, preferred_element_type=jnp.float32
    ) * HEAD_DIM ** (-0.5)
    distance = query_places[:, :, None] - key_places[:, None, :]
    valid = (distance >= 0) & (distance < WINDOW) & (key_places[:, None, :] >= 0)
    valid = valid & (query_docs[:, :, None] == key_docs[:, None, :])
    scores = jnp.where(valid[:, None, None], scores, masked_value)
    sinks = sink_logits.reshape(local_kv, group_size)[None, :, :, None]
    top = jnp.maximum(jnp.max(scores, axis=-1), sinks)
    weight = jnp.exp(scores - top[..., None])
    denom = jnp.sum(weight, axis=-1) + jnp.exp(sinks - top)
    summed = jnp.einsum(
        "bhgqk,bkhd->bqhgd",
        weight.astype(jnp.bfloat16),
        value_blocks,
        preferred_element_type=jnp.float32,
    )
    scale = jnp.transpose(denom, (0, 3, 1, 2))[..., None]
    return (summed / scale).reshape(length, queries.shape[1]).astype(jnp.bfloat16)

MESH = pl.DeviceIdType.MESH
PHASES = 4


def block_kernel(
    levels, mixed, wout, resid, gain_m, gain_b, gain_a, gate, up, down, out,
    full_gate, full_up, full_down, psend, precv, after, normed, hidden, fsend, frecv, fown,
    z_recv, z_up, z_dn, y_send, y_recv, c_send, c_recv, own_sem, x_send, x_recv, f_send, f_recv,
):
    y, s, x = lax.axis_index("grp"), lax.axis_index("sp"), lax.axis_index("tp")
    z, c = s // 2, s % 2
    y_peer, x_peer, c_peer = {"grp": 1 - y}, {"tp": 1 - x}, {"sp": z * 2 + 1 - c}
    above, below = {"sp": jnp.minimum(s + 2, 2 * levels - 1)}, {"sp": jnp.maximum(s - 2, 0)}
    half_rows = gate.shape[0] // 2
    down_rows = down.shape[0] // 2
    width = down.shape[1] // 2
    mine = resid.shape[0]
    dim = resid.shape[1]
    own_rows, peer_rows = pl.ds(pl.multiple_of(x * mine, mine), mine), pl.ds(pl.multiple_of((1 - x) * mine, mine), mine)

    barrier = pltpu.get_barrier_semaphore()

    def greet(device):
        pl.semaphore_signal(barrier, inc=1, device_id=device, device_id_type=MESH)

    greet(y_peer)
    greet(x_peer)
    greet(c_peer)

    @pl.when(z < levels - 1)
    def _():
        greet(above)

    @pl.when(z > 0)
    def _():
        greet(below)

    neighbours = jnp.where(z > 0, 1, 0) + jnp.where(z < levels - 1, 1, 0)
    pl.semaphore_wait(barrier, 3 + neighbours)

    def place(q, zz, cc, hh):
        if q < 2:
            row = pl.multiple_of(((zz * 2 + cc) * 2 + hh) * half_rows, half_rows)
            return (full_gate, full_up)[q].at[pl.ds(row, half_rows), :]
        return full_down.at[
            q - 2, zz, pl.ds(pl.multiple_of(hh * down_rows, down_rows), down_rows), pl.ds(pl.multiple_of(cc * width, width), width)
        ]

    def piece(q, hh):
        if q < 2:
            return (gate, up)[q].at[pl.ds(pl.multiple_of(hh * half_rows, half_rows), half_rows), :]
        return down.at[pl.ds(pl.multiple_of(hh * down_rows, down_rows), down_rows), pl.ds((q - 2) * width, width)]

    def remote(source, target, send, recv, device):
        return pltpu.make_async_remote_copy(
            src_ref=source, dst_ref=target, send_sem=send, recv_sem=recv, device_id=device, device_id_type=MESH
        )

    def upward(q, zz, source):
        return remote(source, place(q, zz, c, y), z_up.at[q, zz], z_recv.at[q, zz], above)

    def downward(q, zz, source):
        return remote(source, place(q, zz, c, y), z_dn.at[q, zz], z_recv.at[q, zz], below)

    def across(q, zz):
        block = place(q, zz, c, y)
        return remote(block, block, y_send.at[q, zz], y_recv.at[q, zz], y_peer)

    def arrived_across(q, zz):
        block = place(q, zz, c, 1 - y)
        return remote(block, block, y_send.at[q, zz], y_recv.at[q, zz], y_peer)

    def beside(q, zz, hh, cc, source=None):
        block = place(q, zz, cc, hh)
        return remote(block if source is None else source, block, c_send.at[q, zz, hh], c_recv.at[q, zz, hh], c_peer)

    def keep(q, hh):
        return pltpu.make_async_copy(piece(q, hh), place(q, z, c, hh), own_sem.at[q, hh])

    def own(q):
        @pl.when(z < levels - 1)
        def _():
            upward(q, z, piece(q, y)).start()

        @pl.when(z > 0)
        def _():
            downward(q, z, piece(q, y)).start()

        for hh in range(2):
            beside(q, z, hh, c, piece(q, hh)).start()
            keep(q, hh).start()

    def from_line(q, t):
        low, high = z - t, z + t

        @pl.when(low >= 0)
        def _():
            upward(q, low, place(q, low, c, y)).wait_recv()

            @pl.when(z < levels - 1)
            def _():
                upward(q, low, place(q, low, c, y)).start()

            across(q, low).start()
            beside(q, low, y, c).start()

        @pl.when(high < levels)
        def _():
            downward(q, high, place(q, high, c, y)).wait_recv()

            @pl.when(z > 0)
            def _():
                downward(q, high, place(q, high, c, y)).start()

            across(q, high).start()
            beside(q, high, y, c).start()

    def from_side(q, t):
        for zz, there in ((z - t, z - t >= 0), (z + t, z + t < levels)):

            @pl.when(there)
            def _(zz=zz):
                arrived_across(q, zz).wait_recv()
                beside(q, zz, 1 - y, c).start()

    def from_partner(q, zz):
        for hh in range(2):
            beside(q, zz, hh, 1 - c).wait_recv()

    def project():
        def tile(j, _):
            cols = pl.ds(pl.multiple_of(j * 256, 256), 256)
            psend[:, cols] = jnp.dot(mixed[peer_rows, :], wout[:, cols], preferred_element_type=jnp.float32).astype(jnp.bfloat16)
            out[:, cols] = jnp.dot(mixed[own_rows, :], wout[:, cols], preferred_element_type=jnp.float32).astype(jnp.bfloat16)
            return 0

        lax.fori_loop(0, dim // 256, tile, 0)

    def sent_projection():
        return remote(psend, precv, x_send.at[0], x_recv.at[0], x_peer)

    def sent_normed(rows):
        return remote(normed.at[rows, :], normed.at[rows, :], x_send.at[1], x_recv.at[1], x_peer)

    step_rows = 32

    def norms():
        def tile(i, _):
            rows = pl.ds(pl.multiple_of(i * step_rows, step_rows), step_rows)
            projected = (out[rows, :].astype(jnp.float32) + precv[rows, :].astype(jnp.float32)).astype(jnp.bfloat16).astype(jnp.float32)
            total = (resid[rows, :].astype(jnp.float32) + rms_scaled(projected, gain_m[...])).astype(jnp.bfloat16)
            after[rows, :] = total
            placed = pl.ds(pl.multiple_of(x * mine + i * step_rows, step_rows), step_rows)
            normed[placed, :] = rms_scaled(total.astype(jnp.float32), gain_b[...]).astype(jnp.bfloat16)
            return 0

        lax.fori_loop(0, mine // step_rows, tile, 0)

    tiles = full_gate.shape[1] // 256

    def gathered(w):
        for hh in range(2):
            keep(w, hh).wait()
        for zz in range(levels):
            from_partner(w, zz)

    def gated(first, last):
        def tile(j, _):
            cols = pl.ds(pl.multiple_of(j * 256, 256), 256)
            g = jnp.dot(normed[...], full_gate[:, cols], preferred_element_type=jnp.float32)
            hidden[:, cols] = (g / (1.0 + jnp.exp(-g))).astype(jnp.bfloat16)
            return 0

        lax.fori_loop(first, last, tile, 0)

    def raised(first, last):
        def tile(j, _):
            cols = pl.ds(pl.multiple_of(j * 256, 256), 256)
            u = jnp.dot(normed[...], full_up[:, cols], preferred_element_type=jnp.float32)
            hidden[:, cols] = (hidden[:, cols].astype(jnp.float32) * u).astype(jnp.bfloat16)
            return 0

        lax.fori_loop(first, last, tile, 0)

    def sent_sum(k, zz):
        return remote(fsend.at[k, zz], frecv.at[k, zz], f_send.at[k, zz], f_recv.at[k, zz], x_peer)

    def lowered(k, zz):
        from_partner(k + 2, zz)
        block = full_down.at[k, zz]
        fsend[k, zz] = jnp.dot(hidden[peer_rows, :], block[...], preferred_element_type=jnp.float32).astype(jnp.bfloat16)
        sent_sum(k, zz).start()
        fown[k, zz] = jnp.dot(hidden[own_rows, :], block[...], preferred_element_type=jnp.float32).astype(jnp.bfloat16)

    def lowered_ring(k, t):
        def one(side, _):
            zz = z - t + 2 * t * side

            @pl.when((zz >= 0) & (zz < levels))
            def _():
                lowered(k, zz)

            return 0

        lax.fori_loop(0, 2, one, 0)

    own(0)
    own(1)
    project()
    sent_projection().start()
    previous = None
    second_gate = (levels - 1) + min(2, levels - 1) - 1
    second_up = second_gate + levels - 1
    last_tick = PHASES * (levels - 1) - 1
    for q in range(PHASES):
        for t in range(1, levels):
            from_line(q, t)
            if previous is not None:
                from_side(*previous)
            previous = (q, t)
            if q == 0 and t == 1:
                own(2)
            if q == 0 and t == min(2, levels - 1):
                sent_projection().wait()
                norms()
                sent_normed(own_rows).start()
            if q == 1 and t == 1:
                own(3)
            tick = q * (levels - 1) + t - 1
            if tick == second_gate:
                sent_normed(own_rows).wait_send()
                sent_normed(peer_rows).wait_recv()
                gathered(0)
            if second_gate <= tick < second_up:
                at, spread = tick - second_gate, second_up - second_gate
                gated(tiles * at // spread, tiles * (at + 1) // spread)
            if tick == second_up:
                gathered(1)
            if second_up <= tick < last_tick:
                at, spread = tick - second_up, last_tick - second_up
                raised(tiles * at // spread, tiles * (at + 1) // spread)
            if tick == last_tick:
                for w in (2, 3):
                    for hh in range(2):
                        keep(w, hh).wait()

                def first_half(zz, _):
                    lowered(0, zz)
                    return 0

                lax.fori_loop(0, levels, first_half, 0)
                lowered(1, z)
                for near in range(1, levels - 1):
                    lowered_ring(1, near)
    from_side(*previous)
    lowered_ring(1, levels - 1)

    def drain(zz, _):
        for k in range(2):
            sent_sum(k, zz).wait()
        for q in range(PHASES):
            for hh in range(2):
                beside(q, zz, hh, c).wait_send()

            @pl.when((zz <= z) & (z < levels - 1))
            def _(q=q):
                upward(q, zz, place(q, zz, c, y)).wait_send()

            @pl.when((zz >= z) & (z > 0))
            def _(q=q):
                downward(q, zz, place(q, zz, c, y)).wait_send()

            @pl.when(zz != z)
            def _(q=q):
                across(q, zz).wait_send()

        return 0

    lax.fori_loop(0, levels, drain, 0)

    def finish(i, _):
        rows = pl.ds(pl.multiple_of(i * step_rows, step_rows), step_rows)
        parts = [
            fown[k, zz, rows, cc * width : (cc + 1) * width].astype(jnp.float32)
            + frecv[k, zz, rows, cc * width : (cc + 1) * width].astype(jnp.float32)
            for zz in range(levels)
            for cc in range(2)
            for k in range(2)
        ]
        ffn_out = jnp.concatenate(parts, axis=1).astype(jnp.bfloat16).astype(jnp.float32)
        out[rows, :] = (after[rows, :].astype(jnp.float32) + 0.5 * rms_scaled(ffn_out, gain_a[...])).astype(jnp.bfloat16)
        return 0

    lax.fori_loop(0, mine // step_rows, finish, 0)


def fused(mixed, head_columns, residual, gain_mixed, gain_before, gain_after, gate_weight, up_weight, down_weight):
    levels = lax.axis_size("sp") // 2
    rows, dim = mixed.shape[0], residual.shape[1]
    mine = residual.shape[0]
    hidden = gate_weight.shape[1]
    half = down_weight.shape[1] // 2
    vmem, whole = pl.BlockSpec(memory_space=pltpu.VMEM), pl.BlockSpec(memory_space=pl.ANY)
    bf16, dma = jnp.bfloat16, pltpu.SemaphoreType.DMA
    return pl.pallas_call(
        functools.partial(block_kernel, levels),
        out_shape=jax.ShapeDtypeStruct((mine, dim), bf16),
        in_specs=[vmem] * 6 + [whole] * 3,
        out_specs=vmem,
        scratch_shapes=[
            pltpu.VMEM((dim, hidden), bf16),
            pltpu.VMEM((dim, hidden), bf16),
            pltpu.VMEM((2, levels, hidden, 2 * half), bf16),
            pltpu.VMEM((mine, dim), bf16),
            pltpu.VMEM((mine, dim), bf16),
            pltpu.VMEM((mine, dim), bf16),
            pltpu.VMEM((rows, dim), bf16),
            pltpu.VMEM((rows, hidden), bf16),
            pltpu.VMEM((2, levels, mine, 2 * half), bf16),
            pltpu.VMEM((2, levels, mine, 2 * half), bf16),
            pltpu.VMEM((2, levels, mine, 2 * half), bf16),
            dma((PHASES, levels)),
            dma((PHASES, levels)),
            dma((PHASES, levels)),
            dma((PHASES, levels)),
            dma((PHASES, levels)),
            dma((PHASES, levels, 2)),
            dma((PHASES, levels, 2)),
            dma((PHASES, 2)),
            dma((2,)),
            dma((2,)),
            dma((2, levels)),
            dma((2, levels)),
        ],
        compiler_params=pltpu.CompilerParams(collective_id=0, has_side_effects=True, vmem_limit_bytes=67043328),
    )(
        mixed, head_columns, residual, gain_mixed[None], gain_before[None], gain_after[None],
        gate_weight, up_weight, down_weight,
    )


def per_device(
    queries,
    key_rows,
    value_rows,
    doc_ids,
    sink_logits,
    out_weight,
    residual,
    gain_mixed,
    gain_before,
    gain_after,
    gate_weight,
    up_weight,
    down_weight,
):
    mixed = attend(queries, key_rows, value_rows, doc_ids, sink_logits)
    head_columns = lax.all_gather(out_weight, "sp", axis=1, tiled=True)
    pairs = lax.axis_size("grp") == 2 and lax.axis_size("tp") == 2
    if pairs and lax.axis_size("sp") % 2 == 0 and lax.axis_size("sp") >= 4:
        return fused(
            mixed, head_columns, residual, gain_mixed, gain_before, gain_after, gate_weight, up_weight, down_weight
        )
    projected = lax.psum_scatter(
        jnp.dot(mixed, head_columns, preferred_element_type=jnp.float32).astype(jnp.bfloat16),
        "tp",
        scatter_dimension=0,
        tiled=True,
    ).astype(jnp.float32)
    projected = stored(projected)
    after = stored(residual.astype(jnp.float32) + rms_scaled(projected, gain_mixed))
    normed = rms_scaled(after, gain_before).astype(jnp.bfloat16)
    full_gate, full_up, full_down = (
        lax.all_gather(gate_weight, "sp", axis=0, tiled=True),
        lax.all_gather(up_weight, "sp", axis=0, tiled=True),
        lax.all_gather(down_weight, "sp", axis=1, tiled=True),
    )
    piece = lax.all_gather(normed, "tp", axis=0, tiled=True)
    gate = jnp.dot(piece, full_gate, preferred_element_type=jnp.float32)
    upward = jnp.dot(piece, full_up, preferred_element_type=jnp.float32)
    hidden = (jax.nn.silu(gate) * upward).astype(jnp.bfloat16)
    ffn_out = stored(
        lax.psum_scatter(
            jnp.dot(hidden, full_down, preferred_element_type=jnp.float32).astype(jnp.bfloat16),
            "tp",
            scatter_dimension=0,
            tiled=True,
        ).astype(jnp.float32)
    )
    return (after + 0.5 * rms_scaled(ffn_out, gain_after)).astype(jnp.bfloat16)


def solution(mesh):
    return jax.shard_map(
        per_device,
        mesh=mesh,
        in_specs=(
            P(("grp", "sp"), "tp"),
            P(("grp", "sp"), "tp"),
            P(("grp", "sp"), "tp"),
            P(("grp", "sp")),
            P("tp"),
            P("tp", "sp"),
            P(("grp", "sp", "tp"), None),
            P(),
            P(),
            P(),
            P("sp", "tp"),
            P("sp", "tp"),
            P("tp", "sp"),
        ),
        out_specs=P(("grp", "sp", "tp"), None),
        check_vma=False,
    )
```

profile of v0, /device:TPU:0, one launch (start us, length us, event | category | flops | bytes accessed | tf_op | source)
XLA Modules:
  0.0 285.1 jit_solution(950706369259637708)
XLA Ops:
  6.5 0.7 all-gather.2.cloned.1.call-update
  7.3 0.7 slice.40
  8.0 2.4 collective-permute-start.1
  10.4 0.8 slice.43
  11.2 5.2 %collective-permute-start.2 = (bf16[128,256]{1,0:T(8,128)(2,1)S(1)}, bf16[128,256]{1,0:T(8,128)(2,1)}, u32[]{:S(2)}, u32[]{:S(2)}) collective-permute-start(bf16[128,256]{1,0:T(8,128)(2,1)S(1)} %slice.43), channel_id=1, source_target_pairs={{0,2},{2,4},{4,6},{6,8},{8,10},{10,12},{12,14},{1,3},{3,5},{5,7},{... | collective-permute-start | bytes 196616 | tf_op jit(solution)/shard_map/ppermute | solution.py:21
  16.4 0.8 slice.36
  17.2 1.3 collective-permute-start
  18.6 1.8 reshape.80
  20.5 1.9 reshape.78
  22.4 1.7 reshape.81
  24.1 1.1 copy.24
  25.3 1.1 copy.20
  26.4 1.0 fusion.20
  27.4 1.0 pad_maximum_fusion
  28.7 1.1 copy.23
  30.1 0.5 copy.19
  30.6 2.3 fusion.2
  33.0 1.7 fusion
  34.8 1.6 fusion.9
  36.4 1.2 copy.43
  37.6 1.7 reshape.82.mixed
  39.3 3.0 %all-gather.2.cloned.1.call-done.wout = bf16[512,2048]{1,0:T(8,128)(2,1)} async-done(((bf16[512,256]{1,0:T(8,128)(2,1)}), bf16[512,2048]{1,0:T(8,128)(2,1)}) %all-gather.2.cloned.1.call-update) | async-done | bytes 2097168 | tf_op jit(solution)/shard_map/all_gather | solution.py:437
  42.2 233.3 %shard_map.127 = bf16[384,2048]{1,0:T(8,128)(2,1)} custom-call(bf16[768,512]{1,0:T(8,128)(2,1)} %reshape.82.mixed, bf16[512,2048]{1,0:T(8,128)(2,1)} %all-gather.2.cloned.1.call-done.wout, bf16[384,2048]{1,0:T(8,128)(2,1)} %resid.1, f32[1,2048]{1,0:T(1,128)} %bitcast.37, f32[1,2048]{1,0:T(1,128)} %bitcast.38, f32[1,2048]{1,0:T(1,128)} %bitcast.39, ...), custom_call_target="tpu_custom_call" | custom-call | tf_op jit(solution)/shard_map/pallas_call | solution.py:384
  275.6 2.7 copy.50
  (33 shorter events, 1.0 us)
Async XLA Ops:
  6.5 15.8 %copy-start.3 = (bf16[768,512]{1,0:T(8,128)(2,1)S(1)}, bf16[768,512]{1,0:T(8,128)(2,1)}, u32[]{:S(2)}) copy-start(bf16[768,512]{1,0:T(8,128)(2,1)} %param.13) | copy-start | bytes 2359300
  6.5 35.7 %all-gather.2.cloned.1.call-start = ((), (), s32[]{:S(2)}) async-start(), calls=%async_computation | async-start | bytes 2359296 | tf_op jit(solution)/shard_map/all_gather | solution.py:437
  7.3 17.9 %copy-start.7 = (f32[8]{0:T(128)S(1)}, f32[8]{0:T(128)}, u32[]{:S(2)}) copy-start(f32[8]{0:T(128)} %param.17) | copy-start | bytes 100
  8.0 18.4 %collective-permute-start.1 = (s32[128]{0:T(128)S(1)}, s32[128]{0:T(128)S(1)}, u32[]{:S(2)}, u32[]{:S(2)}) collective-permute-start(s32[128]{0:T(128)S(1)} %slice.40), channel_id=1, source_target_pairs={{0,2},{2,4},{4,6},{6,8},{8,10},{10,12},{12,14},{1,3},{3,5},{5,7},{... | collective-permute-start | bytes 1544 | tf_op jit(solution)/shard_map/ppermute | solution.py:21
  11.2 16.2 %collective-permute-start.2 = (bf16[128,256]{1,0:T(8,128)(2,1)S(1)}, bf16[128,256]{1,0:T(8,128)(2,1)}, u32[]{:S(2)}, u32[]{:S(2)}) collective-permute-start(bf16[128,256]{1,0:T(8,128)(2,1)S(1)} %slice.43), channel_id=1, source_target_pairs={{0,2},{2,4},{4,6},{6,8},{8,10},{10,12},{12,14},{1,3},{3,5},{5,7},{... | collective-permute-start | bytes 196616 | tf_op jit(solution)/shard_map/ppermute | solution.py:21
  17.2 12.5 %collective-permute-start = (bf16[128,256]{1,0:T(8,128)(2,1)S(1)}, bf16[128,256]{1,0:T(8,128)(2,1)S(1)}, u32[]{:S(2)}, u32[]{:S(2)}) collective-permute-start(bf16[128,256]{1,0:T(8,128)(2,1)S(1)} %slice.36), channel_id=1, source_target_pairs={{0,2},{2,4},{4,6},{6,8},{8,10},{10,12},{12,14},{1,3},{3,5},{5,7},{... | collective-permute-start | bytes 196616 | tf_op jit(solution)/shard_map/ppermute | solution.py:21
  20.5 5.9 %copy-start.6 = (s32[768]{0:T(1024)S(1)}, s32[768]{0:T(1024)}, u32[]{:S(2)}) copy-start(s32[768]{0:T(1024)} %param.16) | copy-start | bytes 9220
  20.5 6.9 %copy-start = (bf16[768,256]{1,0:T(8,128)(2,1)S(1)}, bf16[768,256]{1,0:T(8,128)(2,1)}, u32[]{:S(2)}) copy-start(bf16[768,256]{1,0:T(8,128)(2,1)} %param.14) | copy-start | bytes 1179652
  24.1 5.7 %copy-start.1 = (bf16[768,256]{1,0:T(8,128)(2,1)S(1)}, bf16[768,256]{1,0:T(8,128)(2,1)}, u32[]{:S(2)}) copy-start(bf16[768,256]{1,0:T(8,128)(2,1)} %param.15) | copy-start | bytes 1179652
  27.4 3.3 %copy-start.2 = (bf16[6,128,4,2,64]{4,3,2,1,0:T(2,128)(2,1)S(1)}, bf16[6,128,4,2,64]{4,3,2,1,0:T(2,128)(2,1)}, u32[]{:S(2)}) copy-start(bf16[6,128,4,2,64]{4,3,2,1,0:T(2,128)(2,1)} %reshape.81) | copy-start | bytes 2359300
  28.7 1.9 copy-start.5
  33.0 1.8 copy-start.4
Sparse Core Ops, SparseCore 0:
  8.9 33.2 all-gather.1
where the time goes:
time: 286 us; the launch traced here: 285 us
  Pallas kernels  233 us (81%)
  local copies, waits for them, and re-layouts  17.8 us (6%)
  between operations  13.6 us (5%)
  starting transfers between devices  8.88 us (3%)
  matrix products  3.89 us (1%)
  other arithmetic  3.88 us (1%)
  waiting for transfers between devices  3.68 us (1%)
    pallas_call x1, Pallas kernels, fused(): pl.pallas_call(functools.partial(block_kernel, levels), out_shape=jax.Sha...  233 us
    ppermute x3, starting transfers between devices, passed_along(): lax.ppermute(value, axis, [(source, source + steps) for source in range(f...  8.88 us
    concatenate x8, local copies, waits for them, and re-layouts, windows(): return jnp.concatenate([first, second], axis=1)  8.06 us
  transfers between devices with their start and end apart: 4, of which 1 were waited for; matrix products, arithmetic and copies ran while one was open for 8% of the time, Pallas kernels for 0%

commit v1 on v0

v1 whole, which is shorter than its diff:
```python
import functools

import jax
import jax.numpy as jnp
from jax import lax
from jax.experimental import pallas as pl
from jax.experimental.pallas import tpu as pltpu
from jax.sharding import PartitionSpec as P

HEAD_DIM = 64
WINDOW = 128


epsilon = 1e-06
masked_value = -1e30


def passed_along(value, axis, steps):
    count = lax.axis_size(axis)
    first, last = (max(0, -steps), min(count, count - steps))
    return lax.ppermute(value, axis, [(source, source + steps) for source in range(first, last)])


def stored(value):
    return lax.optimization_barrier(value.astype(jnp.bfloat16)).astype(jnp.float32)


def rms_scaled(value, gain):
    return value * lax.rsqrt(jnp.mean(value * value, axis=-1, keepdims=True) + epsilon) * gain


def windows(array, blocks):
    first = array[:-WINDOW].reshape((blocks, WINDOW) + array.shape[1:])
    second = array[WINDOW:].reshape((blocks, WINDOW) + array.shape[1:])
    return jnp.concatenate([first, second], axis=1)


def attend(queries, key_rows, value_rows, doc_ids, sink_logits):
    length = queries.shape[0]
    blocks = length // WINDOW
    local_kv = key_rows.shape[1] // HEAD_DIM
    group_size = queries.shape[1] // HEAD_DIM // local_kv
    offset = lax.axis_index("sp") * length
    tail_keys, tail_values, tail_docs = passed_along(
        (key_rows[length - WINDOW :], value_rows[length - WINDOW :], doc_ids[length - WINDOW :]),
        "sp",
        1,
    )
    key_blocks = windows(jnp.concatenate([tail_keys, key_rows], axis=0), blocks).reshape(
        blocks, 2 * WINDOW, local_kv, HEAD_DIM
    )
    value_blocks = windows(jnp.concatenate([tail_values, value_rows], axis=0), blocks).reshape(
        blocks, 2 * WINDOW, local_kv, HEAD_DIM
    )
    key_docs = windows(jnp.concatenate([tail_docs, doc_ids], axis=0), blocks)
    key_places = windows(offset - WINDOW + jnp.arange(length + WINDOW, dtype=jnp.int32), blocks)
    query_places = (offset + jnp.arange(length, dtype=jnp.int32)).reshape(blocks, WINDOW)
    query_docs = doc_ids.reshape(blocks, WINDOW)
    query_blocks = queries.reshape(blocks, WINDOW, local_kv, group_size, HEAD_DIM)
    scores = jnp.einsum(
        "bqhgd,bkhd->bhgqk", query_blocks, key_blocks, preferred_element_type=jnp.float32
    ) * HEAD_DIM ** (-0.5)
    distance = query_places[:, :, None] - key_places[:, None, :]
    valid = (distance >= 0) & (distance < WINDOW) & (key_places[:, None, :] >= 0)
    valid = valid & (query_docs[:, :, None] == key_docs[:, None, :])
    scores = jnp.where(valid[:, None, None], scores, masked_value)
    sinks = sink_logits.reshape(local_kv, group_size)[None, :, :, None]
    top = jnp.maximum(jnp.max(scores, axis=-1), sinks)
    weight = jnp.exp(scores - top[..., None])
    denom = jnp.sum(weight, axis=-1) + jnp.exp(sinks - top)
    summed = jnp.einsum(
        "bhgqk,bkhd->bqhgd",
        weight.astype(jnp.bfloat16),
        value_blocks,
        preferred_element_type=jnp.float32,
    )
    scale = jnp.transpose(denom, (0, 3, 1, 2))[..., None]
    return (summed / scale).reshape(length, queries.shape[1]).astype(jnp.bfloat16)

MESH = pl.DeviceIdType.MESH
QUARTERS = 4
SPLIT = 2
LAG = 2
TILE = 256
STEP_ROWS = 32


def block_kernel(
    levels, queries, keys, values, docs, sinks, wout, resid, gain_m, gain_b, gain_a, gate, up, down, out,
    full_out, full_gu, full_down, q_buf, k_buf, v_buf, d_buf, mixed, after, normed, hidden, fsend, frecv, fown,
    local_sem, halo_send, halo_recv, o_send, o_recv, oy_send, oy_recv, oc_send, oc_recv,
    z_recv, z_up, z_dn, y_send, y_recv, c_send, c_recv, x_send, x_recv, f_send, f_recv, out_sem,
):
    y, s, x = lax.axis_index("grp"), lax.axis_index("sp"), lax.axis_index("tp")
    z, c = s // 2, s % 2
    count = 2 * levels
    y_peer, x_peer, c_peer = {"grp": 1 - y}, {"tp": 1 - x}, {"sp": z * 2 + 1 - c}
    above, below = {"sp": jnp.minimum(s + 2, count - 1)}, {"sp": jnp.maximum(s - 2, 0)}
    ahead, behind = {"sp": jnp.minimum(s + 1, count - 1)}, {"sp": jnp.maximum(s - 1, 0)}
    rows, dim, hid = q_buf.shape[0], full_gu.shape[1], full_gu.shape[2]
    mine = after.shape[0]
    blocks = rows // WINDOW
    kv_tiles = k_buf.shape[1] // (2 * HEAD_DIM)
    shard = gate.shape[0]
    half_rows = shard // 2
    out_rows = wout.shape[0] // 2
    out_cols = wout.shape[1]
    down_rows = down.shape[0] // 2
    width = down.shape[1] // 2
    quarter = hid // QUARTERS
    part_rows = down_rows // SPLIT
    chunks, pieces = 2 * QUARTERS, 2 * SPLIT
    own_rows, peer_rows = pl.ds(pl.multiple_of(x * mine, mine), mine), pl.ds(pl.multiple_of((1 - x) * mine, mine), mine)

    barrier = pltpu.get_barrier_semaphore()

    def greet(device):
        pl.semaphore_signal(barrier, inc=1, device_id=device, device_id_type=MESH)

    greet(y_peer)
    greet(x_peer)
    greet(c_peer)

    def greet_line(zz, _):
        @pl.when(zz != z)
        def _():
            greet({"sp": zz * 2 + c})

        return 0

    lax.fori_loop(0, levels, greet_line, 0)

    @pl.when((c == 1) & (z < levels - 1))
    def _():
        greet(ahead)

    @pl.when((c == 0) & (z > 0))
    def _():
        greet(behind)

    def local(source, target, n):
        return pltpu.make_async_copy(source, target, local_sem.at[n])

    shard_rows = pl.ds(pl.multiple_of(s * shard, shard), shard)
    loads = [
        local(wout, full_out.at[:, pl.ds(pl.multiple_of(s * out_cols, out_cols), out_cols)], 0),
        local(keys, k_buf.at[pl.ds(WINDOW, rows), :], 1),
        local(values, v_buf.at[pl.ds(WINDOW, rows), :], 2),
        local(docs, d_buf.at[pl.ds(1, blocks)], 3),
        local(queries, q_buf, 4),
        local(gate, full_gu.at[0, shard_rows, :], 5),
        local(up, full_gu.at[1, shard_rows, :], 6),
        local(down.at[:, pl.ds(0, width)], full_down.at[0, z, :, pl.ds(pl.multiple_of(c * width, width), width)], 7),
        local(down.at[:, pl.ds(width, width)], full_down.at[1, z, :, pl.ds(pl.multiple_of(c * width, width), width)], 8),
        local(resid, after, 9),
    ]
    for load in loads:
        load.start()

    links = jnp.where((c == 1) & (z < levels - 1), 1, 0) + jnp.where((c == 0) & (z > 0), 1, 0)
    pl.semaphore_wait(barrier, 3 + levels - 1 + links)

    def remote(source, target, send, recv, device):
        return pltpu.make_async_remote_copy(
            src_ref=source, dst_ref=target, send_sem=send, recv_sem=recv, device_id=device, device_id_type=MESH
        )

    def halo(n):
        source, target = (
            (keys.at[pl.ds(rows - WINDOW, WINDOW), :], k_buf.at[pl.ds(0, WINDOW), :]),
            (values.at[pl.ds(rows - WINDOW, WINDOW), :], v_buf.at[pl.ds(0, WINDOW), :]),
            (docs.at[pl.ds(blocks - 1, 1)], d_buf.at[pl.ds(0, 1)]),
        )[n]
        return remote(source, target, halo_send.at[n], halo_recv.at[n], ahead)

    @pl.when(s < count - 1)
    def _():
        for n in range(3):
            halo(n).start()

    def out_place(zz, cc, hh):
        column = pl.multiple_of((zz * 2 + cc) * out_cols, out_cols)
        return full_out.at[pl.ds(pl.multiple_of(hh * out_rows, out_rows), out_rows), pl.ds(column, out_cols)]

    def out_line(target, source):
        block = out_place(source, c, y)
        return remote(block, block, o_send.at[target], o_recv.at[source], {"sp": target * 2 + c})

    def out_across(zz, hh):
        block = out_place(zz, c, hh)
        return remote(block, block, oy_send.at[zz], oy_recv.at[zz], y_peer)

    def out_beside(zz, hh, cc):
        block = out_place(zz, cc, hh)
        return remote(block, block, oc_send.at[zz, hh], oc_recv.at[zz, hh], c_peer)

    def others(act):
        def one(zz, _):
            @pl.when(zz != z)
            def _():
                act(zz)

            return 0

        lax.fori_loop(0, levels, one, 0)

    def place(n, zz, cc, hh):
        stage, p = n
        if stage == 0:
            row = pl.multiple_of(((zz * 2 + cc) * 2 + hh) * half_rows, half_rows)
            column = pl.multiple_of((p // 2) * quarter, quarter)
            return full_gu.at[p % 2, pl.ds(row, half_rows), pl.ds(column, quarter)]
        row = pl.multiple_of(hh * down_rows + (p % SPLIT) * part_rows, part_rows)
        return full_down.at[p // SPLIT, zz, pl.ds(row, part_rows), pl.ds(pl.multiple_of(cc * width, width), width)]

    def at(n):
        return n[1] + chunks * n[0]

    def upward(n, zz):
        block = place(n, zz, c, y)
        return remote(block, block, z_up.at[at(n), zz], z_recv.at[at(n), zz], above)

    def downward(n, zz):
        block = place(n, zz, c, y)
        return remote(block, block, z_dn.at[at(n), zz], z_recv.at[at(n), zz], below)

    def across(n, zz, hh):
        block = place(n, zz, c, hh)
        return remote(block, block, y_send.at[at(n), zz], y_recv.at[at(n), zz], y_peer)

    def beside(n, zz, hh, cc):
        block = place(n, zz, cc, hh)
        return remote(block, block, c_send.at[at(n), zz, hh], c_recv.at[at(n), zz, hh], c_peer)

    def own(stage, amount):
        def one(p, _):
            n = (stage, p)

            @pl.when(z < levels - 1)
            def _():
                upward(n, z).start()

            @pl.when(z > 0)
            def _():
                downward(n, z).start()

            for hh in range(2):
                beside(n, z, hh, c).start()
            return 0

        lax.fori_loop(0, amount, one, 0)

    def from_line(n, t):
        low, high = z - t, z + t

        @pl.when(low >= 0)
        def _():
            upward(n, low).wait_recv()

            @pl.when(z < levels - 1)
            def _():
                upward(n, low).start()

            across(n, low, y).start()
            beside(n, low, y, c).start()

        @pl.when(high < levels)
        def _():
            downward(n, high).wait_recv()

            @pl.when(z > 0)
            def _():
                downward(n, high).start()

            across(n, high, y).start()
            beside(n, high, y, c).start()

    def from_side(n, t):
        for zz, there in ((z - t, z - t >= 0), (z + t, z + t < levels)):

            @pl.when(there)
            def _(zz=zz):
                across(n, zz, 1 - y).wait_recv()
                beside(n, zz, 1 - y, c).start()

    def from_partner(n, zz):
        for hh in range(2):
            beside(n, zz, hh, 1 - c).wait_recv()

    low_lane = lax.broadcasted_iota(jnp.int32, (1, 2 * HEAD_DIM), 1) < HEAD_DIM

    def attention(b, _):
        here = pl.ds(pl.multiple_of(b * WINDOW, WINDOW), WINDOW)
        span = pl.ds(pl.multiple_of(b * WINDOW, WINDOW), 2 * WINDOW)
        key_docs = jnp.concatenate([d_buf[b], d_buf[b + 1]], axis=1)
        query_docs = jnp.transpose(jnp.broadcast_to(d_buf[b + 1], (WINDOW, WINDOW)))
        query_docs = jnp.concatenate([query_docs, query_docs], axis=1)
        query_at = lax.broadcasted_iota(jnp.int32, (WINDOW, 2 * WINDOW), 0)
        key_at = lax.broadcasted_iota(jnp.int32, (WINDOW, 2 * WINDOW), 1)
        valid = (key_at > query_at) & (key_at <= query_at + WINDOW) & (query_docs == key_docs)
        for m in range(kv_tiles):
            lanes = slice(m * 2 * HEAD_DIM, (m + 1) * 2 * HEAD_DIM)
            key_tile = k_buf[span, lanes].astype(jnp.float32)
            value_tile = v_buf[span, lanes].astype(jnp.float32)
            key_turned = pltpu.roll(key_tile, HEAD_DIM, 1)
            value_turned = pltpu.roll(value_tile, HEAD_DIM, 1)
            for e in range(2):
                head = 2 * m + e
                first, second = (key_tile, key_turned) if e == 0 else (key_turned, key_tile)
                key_pair = jnp.where(low_lane, first, second).astype(jnp.bfloat16)
                first, second = (value_tile, value_turned) if e == 0 else (value_turned, value_tile)
                value_pair = jnp.where(low_lane, first, second).astype(jnp.bfloat16)
                columns = slice(head * 2 * HEAD_DIM, (head + 1) * 2 * HEAD_DIM)
                query = q_buf[here, columns].astype(jnp.float32) * HEAD_DIM ** (-0.5)
                stacked = jnp.concatenate(
                    [jnp.where(low_lane, query, 0.0), jnp.where(low_lane, 0.0, query)], axis=0
                ).astype(jnp.bfloat16)
                scores = lax.dot_general(
                    stacked, key_pair, (((1,), (1,)), ((), ())), preferred_element_type=jnp.float32
                )
                results = []
                for g in range(2):
                    sink = sinks[2 * head + g]
                    score = jnp.where(valid, scores[g * WINDOW : (g + 1) * WINDOW], masked_value)
                    top = jnp.maximum(jnp.max(score, axis=1, keepdims=True), sink)
                    weight = jnp.exp(score - top)
                    denom = jnp.sum(weight, axis=1, keepdims=True) + jnp.exp(sink - top)
                    summed = jnp.dot(weight.astype(jnp.bfloat16), value_pair, preferred_element_type=jnp.float32)
                    results.append(summed / denom)
                mixed[here, columns] = jnp.where(low_lane, results[0], results[1]).astype(jnp.bfloat16)
        return 0

    def project():
        def tile(j, _):
            cols = pl.ds(pl.multiple_of(j * TILE, TILE), TILE)
            fsend[j] = jnp.dot(mixed[peer_rows, :], full_out[:, cols], preferred_element_type=jnp.float32).astype(jnp.bfloat16)
            fown[j] = jnp.dot(mixed[own_rows, :], full_out[:, cols], preferred_element_type=jnp.float32).astype(jnp.bfloat16)
            return 0

        lax.fori_loop(0, dim // TILE, tile, 0)

    def sent_projection():
        return remote(fsend, frecv, x_send.at[0], x_recv.at[0], x_peer)

    def sent_normed(where):
        return remote(normed.at[where, :], normed.at[where, :], x_send.at[1], x_recv.at[1], x_peer)

    def norms():
        def tile(i, _):
            here = pl.ds(pl.multiple_of(i * STEP_ROWS, STEP_ROWS), STEP_ROWS)
            parts = [fown[j, here, :].astype(jnp.float32) + frecv[j, here, :].astype(jnp.float32) for j in range(dim // TILE)]
            projected = jnp.concatenate(parts, axis=1).astype(jnp.bfloat16).astype(jnp.float32)
            total = (after[here, :].astype(jnp.float32) + rms_scaled(projected, gain_m[...])).astype(jnp.bfloat16)
            after[here, :] = total
            placed = pl.ds(pl.multiple_of(x * mine + i * STEP_ROWS, STEP_ROWS), STEP_ROWS)
            normed[placed, :] = rms_scaled(total.astype(jnp.float32), gain_b[...]).astype(jnp.bfloat16)
            return 0

        lax.fori_loop(0, mine // STEP_ROWS, tile, 0)

    def hidden_tile(j, _):
        cols = pl.ds(pl.multiple_of(j * TILE, TILE), TILE)
        g = jnp.dot(normed[...], full_gu[0, :, cols], preferred_element_type=jnp.float32)
        u = jnp.dot(normed[...], full_gu[1, :, cols], preferred_element_type=jnp.float32)
        hidden[:, cols] = (g / (1.0 + jnp.exp(-g)) * u).astype(jnp.bfloat16)
        return 0

    per_quarter = quarter // TILE

    def tiles_after(g):
        return jnp.where(g % 2 == 1, per_quarter * (g // 2) + (per_quarter + 1) // 2, per_quarter * (g // 2))

    def filled(g):
        def one(zz, _):
            from_partner((0, g), zz)
            return 0

        lax.fori_loop(0, levels, one, 0)

    def sent_sum(n):
        return remote(fsend.at[n], frecv.at[n], f_send.at[n], f_recv.at[n], x_peer)

    def lowered(k, zz):
        for r in range(SPLIT):
            from_partner((1, k * SPLIT + r), zz)
        n = k * levels + zz
        block = full_down.at[k, zz]
        fsend[n] = jnp.dot(hidden[peer_rows, :], block[...], preferred_element_type=jnp.float32).astype(jnp.bfloat16)
        sent_sum(n).start()
        fown[n] = jnp.dot(hidden[own_rows, :], block[...], preferred_element_type=jnp.float32).astype(jnp.bfloat16)

    def ring(k, t):
        def one(side, _):
            zz = z - t + 2 * t * side

            @pl.when((zz >= 0) & (zz < levels))
            def _():
                lowered(k, zz)

            return 0

        lax.fori_loop(0, jnp.where(t == 0, 1, 2), one, 0)

    def side_before(p, t):
        @pl.when(p >= LAG)
        def _():
            from_side((0, p - LAG), t)

        if t > 1:

            @pl.when(p < LAG)
            def _():
                from_side((0, p - LAG + chunks), t - 1)

    def line_steps(t, first, last):
        def one(p, _):
            from_line((0, p), t)
            side_before(p, t)
            return 0

        lax.fori_loop(first, last, one, 0)

    loads[0].wait()
    others(lambda zz: out_line(zz, z).start())
    for hh in range(2):
        out_beside(z, hh, c).start()
    loads[5].wait()
    loads[6].wait()
    own(0, chunks)
    for n in range(1, 5):
        loads[n].wait()

    @pl.when(s == 0)
    def _():
        k_buf[pl.ds(0, WINDOW), :] = jnp.zeros((WINDOW, k_buf.shape[1]), k_buf.dtype)
        v_buf[pl.ds(0, WINDOW), :] = jnp.zeros((WINDOW, v_buf.shape[1]), v_buf.dtype)
        d_buf[0] = jnp.full((1, WINDOW), -1, jnp.int32)

    @pl.when(s > 0)
    def _():
        for n in range(3):
            halo(n).wait_recv()

    lax.fori_loop(0, blocks // 2, attention, 0)

    def out_arrived(zz):
        out_line(z, zz).wait_recv()
        out_across(zz, y).start()
        out_beside(zz, y, c).start()

    others(out_arrived)
    lax.fori_loop(blocks // 2, blocks, attention, 0)
    line_steps(1, 0, 1)

    def out_crossed(zz):
        out_across(zz, 1 - y).wait_recv()
        out_beside(zz, 1 - y, c).start()

    others(out_crossed)
    line_steps(1, 1, 2)

    def out_filled(zz, _):
        for hh in range(2):
            out_beside(zz, hh, 1 - c).wait_recv()
        return 0

    lax.fori_loop(0, levels, out_filled, 0)
    project()
    sent_projection().start()
    line_steps(1, 2, chunks)
    line_steps(2, 0, LAG + 1)
    loads[9].wait()
    sent_projection().wait()
    norms()
    sent_normed(own_rows).start()
    line_steps(2, LAG + 1, chunks)
    for t in range(3, levels - 1):
        line_steps(t, 0, chunks)
    loads[7].wait()
    loads[8].wait()
    own(1, pieces)
    last = levels - 1
    line_steps(last, 0, LAG + 1)
    sent_normed(own_rows).wait_send()
    sent_normed(peer_rows).wait_recv()
    filled(0)

    def gated(p, _):
        from_line((0, p), last)
        from_side((0, p - LAG), last)
        filled(p - LAG)
        lax.fori_loop(tiles_after(p - LAG - 1), tiles_after(p - LAG), hidden_tile, 0)
        return 0

    lax.fori_loop(LAG + 1, chunks, gated, 0)

    def closing(u, _):
        from_line((1, u), 1)
        g = u - LAG + chunks

        @pl.when(u < LAG)
        def _():
            from_side((0, g), last)
            filled(g)

        @pl.when(u >= LAG)
        def _():
            from_side((1, u - LAG), 1)

        done = jnp.where(u < LAG, tiles_after(g), jnp.where(u == LAG, hid // TILE, 0))
        begun = jnp.where(u < LAG, tiles_after(g - 1), jnp.where(u == LAG, tiles_after(chunks - 1), 0))
        lax.fori_loop(begun, done, hidden_tile, 0)
        return 0

    lax.fori_loop(0, pieces, closing, 0)
    lowered(0, z)
    flat = pieces * (levels - 1)

    def settled(v):
        @pl.when(v % SPLIT == SPLIT - 1)
        def _():
            ring((v % pieces) // SPLIT, v // pieces + 1)

    settled(jnp.int32(pieces - LAG - 1))

    def lowering(u, _):
        from_line((1, u % pieces), u // pieces + 1)
        v = u - LAG
        from_side((1, v % pieces), v // pieces + 1)

        @pl.when(u == pieces)
        def _():
            lowered(1, z)

        settled(v)
        return 0

    lax.fori_loop(pieces, flat, lowering, 0)

    def ending(v, _):
        from_side((1, v % pieces), v // pieces + 1)
        settled(v)
        return 0

    lax.fori_loop(flat - LAG, flat, ending, 0)

    @pl.when(s < count - 1)
    def _():
        for n in range(3):
            halo(n).wait_send()

    for hh in range(2):
        out_beside(z, hh, c).wait_send()

    def out_drained(zz):
        out_line(zz, z).wait_send()
        out_across(zz, y).wait_send()
        for hh in range(2):
            out_beside(zz, hh, c).wait_send()

    others(out_drained)

    def drain(zz, _):
        for stage, amount in ((0, chunks), (1, pieces)):

            def one(p, _, stage=stage):
                n = (stage, p)
                for hh in range(2):
                    beside(n, zz, hh, c).wait_send()

                @pl.when((zz <= z) & (z < levels - 1))
                def _():
                    upward(n, zz).wait_send()

                @pl.when((zz >= z) & (z > 0))
                def _():
                    downward(n, zz).wait_send()

                @pl.when(zz != z)
                def _():
                    across(n, zz, y).wait_send()

                return 0

            lax.fori_loop(0, amount, one, 0)
        return 0

    lax.fori_loop(0, levels, drain, 0)

    def sums(n, _):
        sent_sum(n).wait()
        return 0

    lax.fori_loop(0, 2 * levels, sums, 0)

    def finish(i, _):
        here = pl.ds(pl.multiple_of(i * STEP_ROWS, STEP_ROWS), STEP_ROWS)
        parts = [
            fown[k * levels + zz, here, cc * width : (cc + 1) * width].astype(jnp.float32)
            + frecv[k * levels + zz, here, cc * width : (cc + 1) * width].astype(jnp.float32)
            for zz in range(levels)
            for cc in range(2)
            for k in range(2)
        ]
        ffn_out = jnp.concatenate(parts, axis=1).astype(jnp.bfloat16).astype(jnp.float32)
        out[here, :] = (after[here, :].astype(jnp.float32) + 0.5 * rms_scaled(ffn_out, gain_a[...])).astype(jnp.bfloat16)
        return 0

    lax.fori_loop(0, mine // STEP_ROWS, finish, 0)


def fused(
    queries, key_rows, value_rows, doc_ids, sink_logits, out_weight,
    residual, gain_mixed, gain_before, gain_after, gate_weight, up_weight, down_weight,
):
    levels = lax.axis_size("sp") // 2
    rows, dim = queries.shape[0], residual.shape[1]
    blocks = rows // WINDOW
    mine = residual.shape[0]
    hid = gate_weight.shape[1]
    heads = out_weight.shape[0]
    half = down_weight.shape[1] // 2
    vmem, whole = pl.BlockSpec(memory_space=pltpu.VMEM), pl.BlockSpec(memory_space=pl.ANY)
    scalars = pl.BlockSpec(memory_space=pltpu.SMEM)
    bf16, dma = jnp.bfloat16, pltpu.SemaphoreType.DMA
    pieces = 2 * QUARTERS + 2 * SPLIT
    return pl.pallas_call(
        functools.partial(block_kernel, levels),
        out_shape=jax.ShapeDtypeStruct((mine, dim), bf16),
        in_specs=[whole] * 4 + [scalars] + [whole] * 2 + [vmem] * 3 + [whole] * 3,
        out_specs=vmem,
        scratch_shapes=[
            pltpu.VMEM((heads, dim), bf16),
            pltpu.VMEM((2, dim, hid), bf16),
            pltpu.VMEM((2, levels, hid, 2 * half), bf16),
            pltpu.VMEM(queries.shape, bf16),
            pltpu.VMEM((rows + WINDOW, key_rows.shape[1]), bf16),
            pltpu.VMEM((rows + WINDOW, value_rows.shape[1]), bf16),
            pltpu.VMEM((blocks + 1, 1, WINDOW), jnp.int32),
            pltpu.VMEM(queries.shape, bf16),
            pltpu.VMEM((mine, dim), bf16),
            pltpu.VMEM((rows, dim), bf16),
            pltpu.VMEM((rows, hid), bf16),
            pltpu.VMEM((2 * levels, mine, 2 * half), bf16),
            pltpu.VMEM((2 * levels, mine, 2 * half), bf16),
            pltpu.VMEM((2 * levels, mine, 2 * half), bf16),
            dma((10,)),
            dma((3,)),
            dma((3,)),
            dma((levels,)),
            dma((levels,)),
            dma((levels,)),
            dma((levels,)),
            dma((levels, 2)),
            dma((levels, 2)),
            dma((pieces, levels)),
            dma((pieces, levels)),
            dma((pieces, levels)),
            dma((pieces, levels)),
            dma((pieces, levels)),
            dma((pieces, levels, 2)),
            dma((pieces, levels, 2)),
            dma((2,)),
            dma((2,)),
            dma((2 * levels,)),
            dma((2 * levels,)),
            dma((1,)),
        ],
        compiler_params=pltpu.CompilerParams(collective_id=0, has_side_effects=True, vmem_limit_bytes=67043328),
    )(
        queries, key_rows, value_rows, doc_ids.reshape(blocks, 1, WINDOW), sink_logits, out_weight,
        residual, gain_mixed[None], gain_before[None], gain_after[None], gate_weight, up_weight, down_weight,
    )


def per_device(
    queries,
    key_rows,
    value_rows,
    doc_ids,
    sink_logits,
    out_weight,
    residual,
    gain_mixed,
    gain_before,
    gain_after,
    gate_weight,
    up_weight,
    down_weight,
):
    pairs = lax.axis_size("grp") == 2 and lax.axis_size("tp") == 2
    if pairs and lax.axis_size("sp") % 2 == 0 and lax.axis_size("sp") >= 8:
        return fused(
            queries, key_rows, value_rows, doc_ids, sink_logits, out_weight,
            residual, gain_mixed, gain_before, gain_after, gate_weight, up_weight, down_weight,
        )
    mixed = attend(queries, key_rows, value_rows, doc_ids, sink_logits)
    head_columns = lax.all_gather(out_weight, "sp", axis=1, tiled=True)
    projected = lax.psum_scatter(
        jnp.dot(mixed, head_columns, preferred_element_type=jnp.float32).astype(jnp.bfloat16),
        "tp",
        scatter_dimension=0,
        tiled=True,
    ).astype(jnp.float32)
    projected = stored(projected)
    after = stored(residual.astype(jnp.float32) + rms_scaled(projected, gain_mixed))
    normed = rms_scaled(after, gain_before).astype(jnp.bfloat16)
    full_gate, full_up, full_down = (
        lax.all_gather(gate_weight, "sp", axis=0, tiled=True),
        lax.all_gather(up_weight, "sp", axis=0, tiled=True),
        lax.all_gather(down_weight, "sp", axis=1, tiled=True),
    )
    piece = lax.all_gather(normed, "tp", axis=0, tiled=True)
    gate = jnp.dot(piece, full_gate, preferred_element_type=jnp.float32)
    upward = jnp.dot(piece, full_up, preferred_element_type=jnp.float32)
    hidden = (jax.nn.silu(gate) * upward).astype(jnp.bfloat16)
    ffn_out = stored(
        lax.psum_scatter(
            jnp.dot(hidden, full_down, preferred_element_type=jnp.float32).astype(jnp.bfloat16),
            "tp",
            scatter_dimension=0,
            tiled=True,
        ).astype(jnp.float32)
    )
    return (after + 0.5 * rms_scaled(ffn_out, gain_after)).astype(jnp.bfloat16)


def solution(mesh):
    return jax.shard_map(
        per_device,
        mesh=mesh,
        in_specs=(
            P(("grp", "sp"), "tp"),
            P(("grp", "sp"), "tp"),
            P(("grp", "sp"), "tp"),
            P(("grp", "sp")),
            P("tp"),
            P("tp", "sp"),
            P(("grp", "sp", "tp"), None),
            P(),
            P(),
            P(),
            P("sp", "tp"),
            P("sp", "tp"),
            P("tp", "sp"),
        ),
        out_specs=P(("grp", "sp", "tp"), None),
        check_vma=False,
    )
```

time: 286 us -> 227 us (0.79)
  local copies, waits for them, and re-layouts: 17.8 us -> 4 us
  between operations: 13.6 us -> 0.01 us
  Pallas kernels: 233 us -> 223 us
  starting transfers between devices: 8.88 us -> 0 us
  matrix products: 3.89 us -> 0 us
  other arithmetic: 3.88 us -> 0 us
  waiting for transfers between devices: 3.68 us -> 0 us
    pallas_call x1, Pallas kernels: 233 us -> 223 us  [fused(): pl.pallas_call(functools.partial(block_kernel, levels), out_shape=jax.Sha...]
    ppermute x3 -> x0, starting transfers between devices: 8.88 us -> none  [passed_along(): lax.ppermute(value, axis, [(source, source + steps) for source in range(f...]
    concatenate x8 -> x0, local copies, waits for them, and re-layouts: 8.06 us -> none  [windows(): return jnp.concatenate([first, second], axis=1)]
    dot_general x2 -> x0, matrix products: 3.89 us -> none  [the longest x1 2.29 us: attend(): jnp.einsum('bqhgd,bkhd->bhgqk', query_blocks, key_blocks, preferred_eleme...]
    all_gather x1 -> x0, waiting for transfers between devices: 2.96 us -> none  [per_device(): head_columns = lax.all_gather(out_weight, 'sp', axis=1, tiled=True)]
  transfers between devices with their start and end apart: 4 -> 0, of which waited for: 1 -> 0; matrix products, arithmetic and copies ran while one was open for 8% -> 0% of each run, Pallas kernels for 0% -> 0%
where the time goes in v1:
time: 227 us
  Pallas kernels  223 us (98%)
  local copies, waits for them, and re-layouts  4 us (2%)
    pallas_call x1, Pallas kernels, fused(): pl.pallas_call(functools.partial(block_kernel, levels), out_shape=jax.Sha...  223 us

profile of v1, /device:TPU:0, one launch (start us, length us, event | category | flops | bytes accessed | tf_op | source)
XLA Modules:
  0.0 226.9 jit_solution(17504075167137902270)
XLA Ops:
  0.0 1.3 reshape.3.docs
  1.3 222.9 %shard_map.127 = bf16[384,2048]{1,0:T(8,128)(2,1)} custom-call(bf16[768,512]{1,0:T(8,128)(2,1)} %queries.1, bf16[768,256]{1,0:T(8,128)(2,1)} %keys.1, bf16[768,256]{1,0:T(8,128)(2,1)} %values.1, s32[6,1,128]{2,1,0:T(1,128)} %reshape.3.docs, f32[8]{0:T(128)} %sinks.1, bf16[512,256]{1,0:T(8,128)(2,1)} %wout.1, bf16[384,2048]{1,0:T(8,128)(2,1)} %resid.1, ...), custom_call_target="tpu_custom_call" | custom-call | tf_op jit(solution)/shard_map/pallas_call | solution.py:627
  224.2 2.7 %copy.15 = bf16[384,2048]{1,0:T(8,128)(2,1)} copy(bf16[384,2048]{1,0:T(8,128)(2,1)} %shard_map.127) | data formatting | bytes 3145728

commit v2 on v1

--- a/solution.py
+++ b/solution.py
@@ -83,13 +83,15 @@
 LAG = 2
 TILE = 256
 STEP_ROWS = 32
+FINAL_ROWS = 64
+NORMS_AT = 11
 
 
 def block_kernel(
     levels, queries, keys, values, docs, sinks, wout, resid, gain_m, gain_b, gain_a, gate, up, down, out,
-    full_out, full_gu, full_down, q_buf, k_buf, v_buf, d_buf, mixed, after, normed, hidden, fsend, frecv, fown,
-    local_sem, halo_send, halo_recv, o_send, o_recv, oy_send, oy_recv, oc_send, oc_recv,
-    z_recv, z_up, z_dn, y_send, y_recv, c_send, c_recv, x_send, x_recv, f_send, f_recv, out_sem,
+    full_out, full_gu, full_down, q_buf, k_buf, v_buf, d_buf, mixed, after, normed, hidden, fsum, frecv,
+    local_sem, halo_send, halo_recv, o_sent, o_recv, oy_recv, oc_recv,
+    z_recv, z_up, z_dn, y_sent, y_recv, c_sent, c_recv, x_send, x_recv, f_sent, f_recv,
 ):
     y, s, x = lax.axis_index("grp"), lax.axis_index("sp"), lax.axis_index("tp")
     z, c = s // 2, s % 2
@@ -146,7 +148,7 @@
         local(wout, full_out.at[:, pl.ds(pl.multiple_of(s * out_cols, out_cols), out_cols)], 0),
         local(keys, k_buf.at[pl.ds(WINDOW, rows), :], 1),
         local(values, v_buf.at[pl.ds(WINDOW, rows), :], 2),
-        local(docs, d_buf.at[pl.ds(1, blocks)], 3),
+        local(docs, d_buf.at[:, pl.ds(WINDOW, rows)], 3),
         local(queries, q_buf, 4),
         local(gate, full_gu.at[0, shard_rows, :], 5),
         local(up, full_gu.at[1, shard_rows, :], 6),
@@ -169,7 +171,7 @@
         source, target = (
             (keys.at[pl.ds(rows - WINDOW, WINDOW), :], k_buf.at[pl.ds(0, WINDOW), :]),
             (values.at[pl.ds(rows - WINDOW, WINDOW), :], v_buf.at[pl.ds(0, WINDOW), :]),
-            (docs.at[pl.ds(blocks - 1, 1)], d_buf.at[pl.ds(0, 1)]),
+            (docs.at[:, pl.ds(rows - WINDOW, WINDOW)], d_buf.at[:, pl.ds(0, WINDOW)]),
         )[n]
         return remote(source, target, halo_send.at[n], halo_recv.at[n], ahead)
 
@@ -184,15 +186,15 @@
 
     def out_line(target, source):
         block = out_place(source, c, y)
-        return remote(block, block, o_send.at[target], o_recv.at[source], {"sp": target * 2 + c})
+        return remote(block, block, o_sent.at[0], o_recv.at[source], {"sp": target * 2 + c})
 
     def out_across(zz, hh):
         block = out_place(zz, c, hh)
-        return remote(block, block, oy_send.at[zz], oy_recv.at[zz], y_peer)
+        return remote(block, block, o_sent.at[1], oy_recv.at[zz], y_peer)
 
     def out_beside(zz, hh, cc):
         block = out_place(zz, cc, hh)
-        return remote(block, block, oc_send.at[zz, hh], oc_recv.at[zz, hh], c_peer)
+        return remote(block, block, o_sent.at[2], oc_recv.at[0], c_peer)
 
     def others(act):
         def one(zz, _):
@@ -218,19 +220,20 @@
 
     def upward(n, zz):
         block = place(n, zz, c, y)
-        return remote(block, block, z_up.at[at(n), zz], z_recv.at[at(n), zz], above)
+        return remote(block, block, z_up.at[n[0], zz], z_recv.at[at(n), zz], above)
 
     def downward(n, zz):
         block = place(n, zz, c, y)
-        return remote(block, block, z_dn.at[at(n), zz], z_recv.at[at(n), zz], below)
+        return remote(block, block, z_dn.at[n[0], zz], z_recv.at[at(n), zz], below)
 
     def across(n, zz, hh):
         block = place(n, zz, c, hh)
-        return remote(block, block, y_send.at[at(n), zz], y_recv.at[at(n), zz], y_peer)
+        return remote(block, block, y_sent.at[n[0]], y_recv.at[at(n), zz], y_peer)
 
     def beside(n, zz, hh, cc):
         block = place(n, zz, cc, hh)
-        return remote(block, block, c_send.at[at(n), zz, hh], c_recv.at[at(n), zz, hh], c_peer)
+        group = n[1] if n[0] == 0 else chunks + n[1] // SPLIT * levels + zz
+        return remote(block, block, c_sent.at[n[0]], c_recv.at[group], c_peer)
 
     def own(stage, amount):
         def one(p, _):
@@ -275,25 +278,37 @@
             across(n, high, y).start()
             beside(n, high, y, c).start()
 
-    def from_side(n, t):
-        for zz, there in ((z - t, z - t >= 0), (z + t, z + t < levels)):
-
-            @pl.when(there)
-            def _(zz=zz):
-                across(n, zz, 1 - y).wait_recv()
-                beside(n, zz, 1 - y, c).start()
-
-    def from_partner(n, zz):
-        for hh in range(2):
-            beside(n, zz, hh, 1 - c).wait_recv()
+    ends = jnp.minimum(z, levels - 1 - z)
+
+    def side_at(i, amount):
+        paired = i < 2 * ends * amount
+        rest = i - 2 * ends * amount
+        t = jnp.where(paired, i // (2 * amount) + 1, ends + 1 + rest // amount)
+        p = jnp.where(paired, (i % (2 * amount)) // 2, rest % amount)
+        upper = jnp.where(paired, i % 2 == 1, 2 * z < levels)
+        return p, jnp.where(upper, z + t, z - t)
+
+    def from_side(stage, i):
+        p, zz = side_at(i, pieces if stage else chunks)
+        n = (stage, p)
+        across(n, zz, 1 - y).wait_recv()
+        beside(n, zz, 1 - y, c).start()
+
+    def line_step(stage, i):
+        amount = pieces if stage else chunks
+        from_line((stage, i % amount), i // amount + 1)
+
+    def taken(block, semaphore):
+        remote(block, block, semaphore, semaphore, c_peer).wait_recv()
 
     low_lane = lax.broadcasted_iota(jnp.int32, (1, 2 * HEAD_DIM), 1) < HEAD_DIM
 
     def attention(b, _):
         here = pl.ds(pl.multiple_of(b * WINDOW, WINDOW), WINDOW)
         span = pl.ds(pl.multiple_of(b * WINDOW, WINDOW), 2 * WINDOW)
-        key_docs = jnp.concatenate([d_buf[b], d_buf[b + 1]], axis=1)
-        query_docs = jnp.transpose(jnp.broadcast_to(d_buf[b + 1], (WINDOW, WINDOW)))
+        key_docs = d_buf[:, span]
+        own_docs = d_buf[:, pl.ds(pl.multiple_of((b + 1) * WINDOW, WINDOW), WINDOW)]
+        query_docs = jnp.transpose(jnp.broadcast_to(own_docs, (WINDOW, WINDOW)))
         query_docs = jnp.concatenate([query_docs, query_docs], axis=1)
         query_at = lax.broadcasted_iota(jnp.int32, (WINDOW, 2 * WINDOW), 0)
         key_at = lax.broadcasted_iota(jnp.int32, (WINDOW, 2 * WINDOW), 1)
@@ -333,14 +348,13 @@
     def project():
         def tile(j, _):
             cols = pl.ds(pl.multiple_of(j * TILE, TILE), TILE)
-            fsend[j] = jnp.dot(mixed[peer_rows, :], full_out[:, cols], preferred_element_type=jnp.float32).astype(jnp.bfloat16)
-            fown[j] = jnp.dot(mixed[own_rows, :], full_out[:, cols], preferred_element_type=jnp.float32).astype(jnp.bfloat16)
+            fsum[j] = jnp.dot(mixed[...], full_out[:, cols], preferred_element_type=jnp.float32).astype(jnp.bfloat16)
             return 0
 
         lax.fori_loop(0, dim // TILE, tile, 0)
 
     def sent_projection():
-        return remote(fsend, frecv, x_send.at[0], x_recv.at[0], x_peer)
+        return remote(fsum.at[:, peer_rows, :], frecv, x_send.at[0], x_recv.at[0], x_peer)
 
     def sent_normed(where):
         return remote(normed.at[where, :], normed.at[where, :], x_send.at[1], x_recv.at[1], x_peer)
@@ -348,11 +362,11 @@
     def norms():
         def tile(i, _):
             here = pl.ds(pl.multiple_of(i * STEP_ROWS, STEP_ROWS), STEP_ROWS)
-            parts = [fown[j, here, :].astype(jnp.float32) + frecv[j, here, :].astype(jnp.float32) for j in range(dim // TILE)]
+            placed = pl.ds(pl.multiple_of(x * mine + i * STEP_ROWS, STEP_ROWS), STEP_ROWS)
+            parts = [fsum[j, placed, :].astype(jnp.float32) + frecv[j, here, :].astype(jnp.float32) for j in range(dim // TILE)]
             projected = jnp.concatenate(parts, axis=1).astype(jnp.bfloat16).astype(jnp.float32)
             total = (after[here, :].astype(jnp.float32) + rms_scaled(projected, gain_m[...])).astype(jnp.bfloat16)
             after[here, :] = total
-            placed = pl.ds(pl.multiple_of(x * mine + i * STEP_ROWS, STEP_ROWS), STEP_ROWS)
             normed[placed, :] = rms_scaled(total.astype(jnp.float32), gain_b[...]).astype(jnp.bfloat16)
             return 0
 
@@ -366,56 +380,40 @@
         return 0
 
     per_quarter = quarter // TILE
-
-    def tiles_after(g):
-        return jnp.where(g % 2 == 1, per_quarter * (g // 2) + (per_quarter + 1) // 2, per_quarter * (g // 2))
+    gathers, lowers = (levels - 1) * chunks, (levels - 1) * pieces
 
     def filled(g):
-        def one(zz, _):
-            from_partner((0, g), zz)
-            return 0
-
-        lax.fori_loop(0, levels, one, 0)
+        columns = pl.ds(pl.multiple_of((g // 2) * quarter, quarter), quarter)
+        taken(full_gu.at[g % 2, pl.ds(0, dim // 2), columns], c_recv.at[g])
+
+    def tiles_by(g):
+        return jnp.minimum(2 * (g - 1), per_quarter * ((g + 1) // 2))
 
     def sent_sum(n):
-        return remote(fsend.at[n], frecv.at[n], f_send.at[n], f_recv.at[n], x_peer)
+        return remote(fsum.at[n, peer_rows, :], frecv.at[n], f_sent.at[0], f_recv.at[0], x_peer)
 
     def lowered(k, zz):
-        for r in range(SPLIT):
-            from_partner((1, k * SPLIT + r), zz)
         n = k * levels + zz
         block = full_down.at[k, zz]
-        fsend[n] = jnp.dot(hidden[peer_rows, :], block[...], preferred_element_type=jnp.float32).astype(jnp.bfloat16)
+        taken(block.at[:, pl.ds(pl.multiple_of((1 - c) * width, width), width)], c_recv.at[chunks + n])
+        fsum[n] = jnp.dot(hidden[...], block[...], preferred_element_type=jnp.float32).astype(jnp.bfloat16)
         sent_sum(n).start()
-        fown[n] = jnp.dot(hidden[own_rows, :], block[...], preferred_element_type=jnp.float32).astype(jnp.bfloat16)
-
-    def ring(k, t):
-        def one(side, _):
-            zz = z - t + 2 * t * side
-
-            @pl.when((zz >= 0) & (zz < levels))
+
+    def settled(v):
+        p, zz = side_at(v, pieces)
+
+        @pl.when(p % SPLIT == SPLIT - 1)
+        def _():
+            lowered(p // SPLIT, zz)
+
+    def steps(first, last):
+        def one(i, _):
+            line_step(0, i)
+
+            @pl.when(i >= LAG)
             def _():
-                lowered(k, zz)
-
-            return 0
-
-        lax.fori_loop(0, jnp.where(t == 0, 1, 2), one, 0)
-
-    def side_before(p, t):
-        @pl.when(p >= LAG)
-        def _():
-            from_side((0, p - LAG), t)
-
-        if t > 1:
-
-            @pl.when(p < LAG)
-            def _():
-                from_side((0, p - LAG + chunks), t - 1)
-
-    def line_steps(t, first, last):
-        def one(p, _):
-            from_line((0, p), t)
-            side_before(p, t)
+                from_side(0, i - LAG)
+
             return 0
 
         lax.fori_loop(first, last, one, 0)
@@ -434,169 +432,135 @@
     def _():
         k_buf[pl.ds(0, WINDOW), :] = jnp.zeros((WINDOW, k_buf.shape[1]), k_buf.dtype)
         v_buf[pl.ds(0, WINDOW), :] = jnp.zeros((WINDOW, v_buf.shape[1]), v_buf.dtype)
-        d_buf[0] = jnp.full((1, WINDOW), -1, jnp.int32)
+        d_buf[:, pl.ds(0, WINDOW)] = jnp.full((1, WINDOW), -1, jnp.int32)
 
     @pl.when(s > 0)
     def _():
         for n in range(3):
             halo(n).wait_recv()
 
-    lax.fori_loop(0, blocks // 2, attention, 0)
-
-    def out_arrived(zz):
-        out_line(z, zz).wait_recv()
-        out_across(zz, y).start()
-        out_beside(zz, y, c).start()
-
-    others(out_arrived)
-    lax.fori_loop(blocks // 2, blocks, attention, 0)
-    line_steps(1, 0, 1)
+    def out_arrived(t):
+        for zz, there in ((z - t, z - t >= 0), (z + t, z + t < levels)):
+
+            @pl.when(there)
+            def _(zz=zz):
+                out_line(z, zz).wait_recv()
+                out_across(zz, y).start()
+                out_beside(zz, y, c).start()
+
+    def out_steps(t, _):
+        attended(t + 2)
+        out_arrived(t)
+        return 0
+
+    def attended(n):
+        lax.fori_loop(blocks * n // (levels + 2), blocks * (n + 1) // (levels + 2), attention, 0)
+
+    lax.fori_loop(0, 3, lambda n, _: (attended(n), 0)[1], 0)
+    lax.fori_loop(1, levels, out_steps, 0)
+    steps(0, 1)
 
     def out_crossed(zz):
         out_across(zz, 1 - y).wait_recv()
         out_beside(zz, 1 - y, c).start()
 
     others(out_crossed)
-    line_steps(1, 1, 2)
-
-    def out_filled(zz, _):
-        for hh in range(2):
-            out_beside(zz, hh, 1 - c).wait_recv()
-        return 0
-
-    lax.fori_loop(0, levels, out_filled, 0)
+    steps(1, 2)
+    taken(full_out.at[:, pl.ds(0, dim // 2)], oc_recv.at[0])
     project()
     sent_projection().start()
-    line_steps(1, 2, chunks)
-    line_steps(2, 0, LAG + 1)
+    steps(2, NORMS_AT)
     loads[9].wait()
     sent_projection().wait()
     norms()
     sent_normed(own_rows).start()
-    line_steps(2, LAG + 1, chunks)
-    for t in range(3, levels - 1):
-        line_steps(t, 0, chunks)
+    second = (levels - 2) * chunks
+    steps(NORMS_AT, second)
     loads[7].wait()
     loads[8].wait()
     own(1, pieces)
-    last = levels - 1
-    line_steps(last, 0, LAG + 1)
+    steps(second, second + LAG + 2)
     sent_normed(own_rows).wait_send()
     sent_normed(peer_rows).wait_recv()
     filled(0)
-
-    def gated(p, _):
-        from_line((0, p), last)
-        from_side((0, p - LAG), last)
-        filled(p - LAG)
-        lax.fori_loop(tiles_after(p - LAG - 1), tiles_after(p - LAG), hidden_tile, 0)
-        return 0
-
-    lax.fori_loop(LAG + 1, chunks, gated, 0)
-
-    def closing(u, _):
-        from_line((1, u), 1)
-        g = u - LAG + chunks
-
-        @pl.when(u < LAG)
-        def _():
-            from_side((0, g), last)
-            filled(g)
-
-        @pl.when(u >= LAG)
-        def _():
-            from_side((1, u - LAG), 1)
-
-        done = jnp.where(u < LAG, tiles_after(g), jnp.where(u == LAG, hid // TILE, 0))
-        begun = jnp.where(u < LAG, tiles_after(g - 1), jnp.where(u == LAG, tiles_after(chunks - 1), 0))
-        lax.fori_loop(begun, done, hidden_tile, 0)
-        return 0
-
-    lax.fori_loop(0, pieces, closing, 0)
-    lowered(0, z)
-    flat = pieces * (levels - 1)
-
-    def settled(v):
-        @pl.when(v % SPLIT == SPLIT - 1)
-        def _():
-            ring((v % pieces) // SPLIT, v // pieces + 1)
-
-    settled(jnp.int32(pieces - LAG - 1))
+    filled(1)
+
+    def gated(g, _):
+        @pl.when(g + LAG < chunks)
+        def _():
+            line_step(0, second + g + LAG)
+
+        @pl.when(g + LAG >= chunks)
+        def _():
+            line_step(1, g + LAG - chunks)
+
+        from_side(0, second + g)
+        filled(g)
+        lax.fori_loop(tiles_by(g - 1), jnp.where(g == chunks - 1, hid // TILE, tiles_by(g)), hidden_tile, 0)
+        return 0
+
+    lax.fori_loop(2, chunks, gated, 0)
 
     def lowering(u, _):
-        from_line((1, u % pieces), u // pieces + 1)
-        v = u - LAG
-        from_side((1, v % pieces), v // pieces + 1)
-
-        @pl.when(u == pieces)
-        def _():
-            lowered(1, z)
-
+        line_step(1, u)
+        from_side(1, u - LAG)
+
+        @pl.when(u < LAG + 2)
+        def _():
+            lowered(u - LAG, z)
+
+        settled(u - LAG)
+        return 0
+
+    lax.fori_loop(LAG, lowers, lowering, 0)
+
+    def ending(v, _):
+        from_side(1, v)
         settled(v)
         return 0
 
-    lax.fori_loop(pieces, flat, lowering, 0)
-
-    def ending(v, _):
-        from_side((1, v % pieces), v // pieces + 1)
-        settled(v)
-        return 0
-
-    lax.fori_loop(flat - LAG, flat, ending, 0)
+    lax.fori_loop(lowers - LAG, lowers, ending, 0)
 
     @pl.when(s < count - 1)
     def _():
         for n in range(3):
             halo(n).wait_send()
 
-    for hh in range(2):
-        out_beside(z, hh, c).wait_send()
-
-    def out_drained(zz):
-        out_line(zz, z).wait_send()
-        out_across(zz, y).wait_send()
-        for hh in range(2):
-            out_beside(zz, hh, c).wait_send()
-
-    others(out_drained)
+    def left(block, semaphore):
+        remote(block, block, semaphore, semaphore, c_peer).wait_send()
+
+    for n in range(2):
+        left(full_out.at[pl.ds(0, out_rows), pl.ds(0, (levels - 1) * out_cols)], o_sent.at[n])
+    left(full_out.at[:, pl.ds(0, dim // 2)], o_sent.at[2])
+    left(full_gu.at[0, pl.ds(0, (levels - 1) * shard), :], y_sent.at[0])
+    left(full_down.at[0, pl.ds(0, levels - 1), pl.ds(0, down_rows), :], y_sent.at[1])
+    left(full_gu.at[0], c_sent.at[0])
+    left(full_down.at[:, :, :, pl.ds(0, width)], c_sent.at[1])
 
     def drain(zz, _):
-        for stage, amount in ((0, chunks), (1, pieces)):
-
-            def one(p, _, stage=stage):
-                n = (stage, p)
-                for hh in range(2):
-                    beside(n, zz, hh, c).wait_send()
-
-                @pl.when((zz <= z) & (z < levels - 1))
-                def _():
-                    upward(n, zz).wait_send()
-
-                @pl.when((zz >= z) & (z > 0))
-                def _():
-                    downward(n, zz).wait_send()
-
-                @pl.when(zz != z)
-                def _():
-                    across(n, zz, y).wait_send()
-
-                return 0
-
-            lax.fori_loop(0, amount, one, 0)
+        def one(sent):
+            left(full_gu.at[0, pl.ds(0, shard), :], sent.at[0, zz])
+            left(full_down.at[0, zz, pl.ds(0, down_rows), :], sent.at[1, zz])
+
+        @pl.when((zz <= z) & (z < levels - 1))
+        def _():
+            one(z_up)
+
+        @pl.when((zz >= z) & (z > 0))
+        def _():
+            one(z_dn)
+
         return 0
 
     lax.fori_loop(0, levels, drain, 0)
-
-    def sums(n, _):
-        sent_sum(n).wait()
-        return 0
-
-    lax.fori_loop(0, 2 * levels, sums, 0)
+    left(frecv, f_sent.at[0])
+    taken(frecv, f_recv.at[0])
 
     def finish(i, _):
-        here = pl.ds(pl.multiple_of(i * STEP_ROWS, STEP_ROWS), STEP_ROWS)
+        here = pl.ds(pl.multiple_of(i * FINAL_ROWS, FINAL_ROWS), FINAL_ROWS)
+        placed = pl.ds(pl.multiple_of(x * mine + i * FINAL_ROWS, FINAL_ROWS), FINAL_ROWS)
         parts = [
-            fown[k * levels + zz, here, cc * width : (cc + 1) * width].astype(jnp.float32)
+            fsum[k * levels + zz, placed, cc * width : (cc + 1) * width].astype(jnp.float32)
             + frecv[k * levels + zz, here, cc * width : (cc + 1) * width].astype(jnp.float32)
             for zz in range(levels)
             for cc in range(2)
@@ -606,7 +570,7 @@
         out[here, :] = (after[here, :].astype(jnp.float32) + 0.5 * rms_scaled(ffn_out, gain_a[...])).astype(jnp.bfloat16)
         return 0
 
-    lax.fori_loop(0, mine // STEP_ROWS, finish, 0)
+    lax.fori_loop(0, mine // FINAL_ROWS, finish, 0)
 
 
 def fused(
@@ -615,7 +579,6 @@
 ):
     levels = lax.axis_size("sp") // 2
     rows, dim = queries.shape[0], residual.shape[1]
-    blocks = rows // WINDOW
     mine = residual.shape[0]
     hid = gate_weight.shape[1]
     heads = out_weight.shape[0]
@@ -636,39 +599,35 @@
             pltpu.VMEM(queries.shape, bf16),
             pltpu.VMEM((rows + WINDOW, key_rows.shape[1]), bf16),
             pltpu.VMEM((rows + WINDOW, value_rows.shape[1]), bf16),
-            pltpu.VMEM((blocks + 1, 1, WINDOW), jnp.int32),
+            pltpu.VMEM((1, rows + WINDOW), jnp.int32),
             pltpu.VMEM(queries.shape, bf16),
             pltpu.VMEM((mine, dim), bf16),
             pltpu.VMEM((rows, dim), bf16),
             pltpu.VMEM((rows, hid), bf16),
-            pltpu.VMEM((2 * levels, mine, 2 * half), bf16),
-            pltpu.VMEM((2 * levels, mine, 2 * half), bf16),
+            pltpu.VMEM((2 * levels, rows, 2 * half), bf16),
             pltpu.VMEM((2 * levels, mine, 2 * half), bf16),
             dma((10,)),
             dma((3,)),
             dma((3,)),
+            dma((3,)),
             dma((levels,)),
             dma((levels,)),
-            dma((levels,)),
-            dma((levels,)),
-            dma((levels, 2)),
-            dma((levels, 2)),
+            dma((1,)),
             dma((pieces, levels)),
+            dma((2, levels)),
+            dma((2, levels)),
+            dma((2,)),
             dma((pieces, levels)),
-            dma((pieces, levels)),
-            dma((pieces, levels)),
-            dma((pieces, levels)),
-            dma((pieces, levels, 2)),
-            dma((pieces, levels, 2)),
+            dma((2,)),
+            dma((2 * QUARTERS + 2 * levels,)),
             dma((2,)),
             dma((2,)),
-            dma((2 * levels,)),
-            dma((2 * levels,)),
+            dma((1,)),
             dma((1,)),
         ],
         compiler_params=pltpu.CompilerParams(collective_id=0, has_side_effects=True, vmem_limit_bytes=67043328),
     )(
-        queries, key_rows, value_rows, doc_ids.reshape(blocks, 1, WINDOW), sink_logits, out_weight,
+        queries, key_rows, value_rows, doc_ids[None], sink_logits, out_weight,
         residual, gain_mixed[None], gain_before[None], gain_after[None], gate_weight, up_weight, down_weight,
     )
 

time: 227 us -> 197 us (0.87)
  Pallas kernels: 223 us -> 191 us
    pallas_call x1, Pallas kernels: 223 us -> 191 us  [fused(): pl.pallas_call(functools.partial(block_kernel, levels), out_shape=jax.Sha...]
where the time goes in v2:
time: 197 us; the launch traced here: 195 us
  Pallas kernels  191 us (97%)
  local copies, waits for them, and re-layouts  3.99 us (2%)
    pallas_call x1, Pallas kernels, fused(): pl.pallas_call(functools.partial(block_kernel, levels), out_shape=jax.Sha...  191 us

profile of v2, /device:TPU:0, one launch (start us, length us, event | category | flops | bytes accessed | tf_op | source)
XLA Modules:
  0.0 195.5 jit_solution(16675792816967481364)
XLA Ops:
  0.0 1.3 broadcast_in_dim.12.docs
  1.3 191.5 %shard_map.127 = bf16[384,2048]{1,0:T(8,128)(2,1)} custom-call(bf16[768,512]{1,0:T(8,128)(2,1)} %queries.1, bf16[768,256]{1,0:T(8,128)(2,1)} %keys.1, bf16[768,256]{1,0:T(8,128)(2,1)} %values.1, s32[1,768]{1,0:T(1,128)} %broadcast_in_dim.12.docs, f32[8]{0:T(128)} %sinks.1, bf16[512,256]{1,0:T(8,128)(2,1)} %wout.1, bf16[384,2048]{1,0:T(8,128)(2,1)} %resid.1, ...), custom_call_target="tpu_custom_call" | custom-call | tf_op jit(solution)/shard_map/pallas_call | solution.py:590
  192.8 2.7 %copy.15 = bf16[384,2048]{1,0:T(8,128)(2,1)} copy(bf16[384,2048]{1,0:T(8,128)(2,1)} %shard_map.127) | data formatting | bytes 3145728

commit v3 on v2

--- a/solution.py
+++ b/solution.py
@@ -79,11 +79,12 @@
 
 MESH = pl.DeviceIdType.MESH
 QUARTERS = 4
-SPLIT = 2
+SPLIT = 4
 LAG = 2
 TILE = 256
 STEP_ROWS = 32
 FINAL_ROWS = 64
+WHOLE = 1
 NORMS_AT = 11
 
 
@@ -91,7 +92,7 @@
     levels, queries, keys, values, docs, sinks, wout, resid, gain_m, gain_b, gain_a, gate, up, down, out,
     full_out, full_gu, full_down, q_buf, k_buf, v_buf, d_buf, mixed, after, normed, hidden, fsum, frecv,
     local_sem, halo_send, halo_recv, o_sent, o_recv, oy_recv, oc_recv,
-    z_recv, z_up, z_dn, y_sent, y_recv, c_sent, c_recv, x_send, x_recv, f_sent, f_recv,
+    z_recv, z_up, z_dn, w_recv, w_sent, y_sent, y_recv, c_sent, c_recv, x_send, x_recv, f_sent, f_recv,
 ):
     y, s, x = lax.axis_index("grp"), lax.axis_index("sp"), lax.axis_index("tp")
     z, c = s // 2, s % 2
@@ -148,7 +149,7 @@
         local(wout, full_out.at[:, pl.ds(pl.multiple_of(s * out_cols, out_cols), out_cols)], 0),
         local(keys, k_buf.at[pl.ds(WINDOW, rows), :], 1),
         local(values, v_buf.at[pl.ds(WINDOW, rows), :], 2),
-        local(docs, d_buf.at[:, pl.ds(WINDOW, rows)], 3),
+        local(docs, d_buf.at[pl.ds(WINDOW, rows)], 3),
         local(queries, q_buf, 4),
         local(gate, full_gu.at[0, shard_rows, :], 5),
         local(up, full_gu.at[1, shard_rows, :], 6),
@@ -171,7 +172,7 @@
         source, target = (
             (keys.at[pl.ds(rows - WINDOW, WINDOW), :], k_buf.at[pl.ds(0, WINDOW), :]),
             (values.at[pl.ds(rows - WINDOW, WINDOW), :], v_buf.at[pl.ds(0, WINDOW), :]),
-            (docs.at[:, pl.ds(rows - WINDOW, WINDOW)], d_buf.at[:, pl.ds(0, WINDOW)]),
+            (docs.at[pl.ds(rows - WINDOW, WINDOW)], d_buf.at[pl.ds(0, WINDOW)]),
         )[n]
         return remote(source, target, halo_send.at[n], halo_recv.at[n], ahead)
 
@@ -228,7 +229,14 @@
 
     def across(n, zz, hh):
         block = place(n, zz, c, hh)
-        return remote(block, block, y_sent.at[n[0]], y_recv.at[at(n), zz], y_peer)
+        return remote(block, block, y_sent.at[0 if n[0] == 0 else 1 + zz], y_recv.at[at(n), zz], y_peer)
+
+    def whole(p, side, source, device):
+        block = place((1, p), source, c, 1 - y)
+        return remote(block, block, w_sent.at[side], w_recv.at[p, side], device)
+
+    def whole_from(p, side):
+        return whole(p, side, z - 1 + 2 * side, above)
 
     def beside(n, zz, hh, cc):
         block = place(n, zz, cc, hh)
@@ -249,12 +257,24 @@
 
             for hh in range(2):
                 beside(n, z, hh, c).start()
+
+            if stage:
+
+                @pl.when((p < WHOLE) & (z < levels - 1))
+                def _():
+                    whole(p, 0, z, above).start()
+
+                @pl.when((p < WHOLE) & (z > 0))
+                def _():
+                    whole(p, 1, z, below).start()
+
             return 0
 
         lax.fori_loop(0, amount, one, 0)
 
     def from_line(n, t):
         low, high = z - t, z + t
+        direct = (n[0] == 1) & (t == 1) & (n[1] < WHOLE)
 
         @pl.when(low >= 0)
         def _():
@@ -264,8 +284,7 @@
             def _():
                 upward(n, low).start()
 
-            across(n, low, y).start()
-            beside(n, low, y, c).start()
+            relayed(n, low, 0, direct)
 
         @pl.when(high < levels)
         def _():
@@ -275,8 +294,22 @@
             def _():
                 downward(n, high).start()
 
-            across(n, high, y).start()
-            beside(n, high, y, c).start()
+            relayed(n, high, 1, direct)
+
+    def relayed(n, zz, side, direct):
+        beside(n, zz, y, c).start()
+        if n[0] == 0:
+            across(n, zz, y).start()
+            return
+
+        @pl.when(jnp.logical_not(direct))
+        def _():
+            across(n, zz, y).start()
+
+        @pl.when(direct)
+        def _():
+            whole_from(jnp.minimum(n[1], WHOLE - 1), side).wait_recv()
+            beside(n, zz, 1 - y, c).start()
 
     ends = jnp.minimum(z, levels - 1 - z)
 
@@ -291,8 +324,16 @@
     def from_side(stage, i):
         p, zz = side_at(i, pieces if stage else chunks)
         n = (stage, p)
-        across(n, zz, 1 - y).wait_recv()
-        beside(n, zz, 1 - y, c).start()
+
+        def one():
+            across(n, zz, 1 - y).wait_recv()
+            beside(n, zz, 1 - y, c).start()
+
+        if stage == 0:
+            one()
+        else:
+            near = (zz - z == 1) | (z - zz == 1)
+            pl.when(jnp.logical_not(near & (p < WHOLE)))(one)
 
     def line_step(stage, i):
         amount = pieces if stage else chunks
@@ -306,8 +347,8 @@
     def attention(b, _):
         here = pl.ds(pl.multiple_of(b * WINDOW, WINDOW), WINDOW)
         span = pl.ds(pl.multiple_of(b * WINDOW, WINDOW), 2 * WINDOW)
-        key_docs = d_buf[:, span]
-        own_docs = d_buf[:, pl.ds(pl.multiple_of((b + 1) * WINDOW, WINDOW), WINDOW)]
+        key_docs = d_buf[span][None]
+        own_docs = d_buf[pl.ds(pl.multiple_of((b + 1) * WINDOW, WINDOW), WINDOW)][None]
         query_docs = jnp.transpose(jnp.broadcast_to(own_docs, (WINDOW, WINDOW)))
         query_docs = jnp.concatenate([query_docs, query_docs], axis=1)
         query_at = lax.broadcasted_iota(jnp.int32, (WINDOW, 2 * WINDOW), 0)
@@ -387,7 +428,7 @@
         taken(full_gu.at[g % 2, pl.ds(0, dim // 2), columns], c_recv.at[g])
 
     def tiles_by(g):
-        return jnp.minimum(2 * (g - 1), per_quarter * ((g + 1) // 2))
+        return jnp.maximum(per_quarter * (g // 2) - jnp.where(g % 2 == 0, per_quarter // 2, 0), 0)
 
     def sent_sum(n):
         return remote(fsum.at[n, peer_rows, :], frecv.at[n], f_sent.at[0], f_recv.at[0], x_peer)
@@ -419,7 +460,17 @@
         lax.fori_loop(first, last, one, 0)
 
     loads[0].wait()
-    others(lambda zz: out_line(zz, z).start())
+
+    def out_sent(t, _):
+        for zz, there in ((z - t, z - t >= 0), (z + t, z + t < levels)):
+
+            @pl.when(there)
+            def _(zz=zz):
+                out_line(zz, z).start()
+
+        return 0
+
+    lax.fori_loop(1, levels, out_sent, 0)
     for hh in range(2):
         out_beside(z, hh, c).start()
     loads[5].wait()
@@ -432,7 +483,7 @@
     def _():
         k_buf[pl.ds(0, WINDOW), :] = jnp.zeros((WINDOW, k_buf.shape[1]), k_buf.dtype)
         v_buf[pl.ds(0, WINDOW), :] = jnp.zeros((WINDOW, v_buf.shape[1]), v_buf.dtype)
-        d_buf[:, pl.ds(0, WINDOW)] = jnp.full((1, WINDOW), -1, jnp.int32)
+        d_buf[pl.ds(0, WINDOW)] = jnp.full((WINDOW,), -1, jnp.int32)
 
     @pl.when(s > 0)
     def _():
@@ -483,7 +534,8 @@
     sent_normed(own_rows).wait_send()
     sent_normed(peer_rows).wait_recv()
     filled(0)
-    filled(1)
+    ratio = half_rows * quarter // (part_rows * width)
+    behind_by = LAG * ratio
 
     def gated(g, _):
         @pl.when(g + LAG < chunks)
@@ -492,34 +544,48 @@
 
         @pl.when(g + LAG >= chunks)
         def _():
-            line_step(1, g + LAG - chunks)
+            for r in range(ratio):
+                line_step(1, (g + LAG - chunks) * ratio + r)
 
         from_side(0, second + g)
-        filled(g)
-        lax.fori_loop(tiles_by(g - 1), jnp.where(g == chunks - 1, hid // TILE, tiles_by(g)), hidden_tile, 0)
+        filled(g - 1)
+        lax.fori_loop(jnp.where(g == 2, 0, tiles_by(g - 1)), tiles_by(g), hidden_tile, 0)
         return 0
 
     lax.fori_loop(2, chunks, gated, 0)
+    ready = tiles_by(chunks - 1)
+    rest = hid // TILE - ready
 
     def lowering(u, _):
         line_step(1, u)
-        from_side(1, u - LAG)
-
-        @pl.when(u < LAG + 2)
-        def _():
-            lowered(u - LAG, z)
-
-        settled(u - LAG)
-        return 0
-
-    lax.fori_loop(LAG, lowers, lowering, 0)
+        v = u - behind_by
+        from_side(1, v)
+
+        @pl.when(v == 0)
+        def _():
+            filled(chunks - 1)
+
+        lax.fori_loop(jnp.minimum(ready + v, hid // TILE), jnp.minimum(ready + v + 1, hid // TILE), hidden_tile, 0)
+
+        @pl.when((v > rest) & (v <= rest + 2))
+        def _():
+            lowered(v - rest - 1, z)
+
+        @pl.when(v > 0)
+        def _():
+            settled(v - 1)
+
+        return 0
+
+    lax.fori_loop(behind_by, lowers, lowering, 0)
 
     def ending(v, _):
         from_side(1, v)
-        settled(v)
-        return 0
-
-    lax.fori_loop(lowers - LAG, lowers, ending, 0)
+        settled(v - 1)
+        return 0
+
+    lax.fori_loop(lowers - behind_by, lowers, ending, 0)
+    settled(jnp.int32(lowers - 1))
 
     @pl.when(s < count - 1)
     def _():
@@ -533,7 +599,6 @@
         left(full_out.at[pl.ds(0, out_rows), pl.ds(0, (levels - 1) * out_cols)], o_sent.at[n])
     left(full_out.at[:, pl.ds(0, dim // 2)], o_sent.at[2])
     left(full_gu.at[0, pl.ds(0, (levels - 1) * shard), :], y_sent.at[0])
-    left(full_down.at[0, pl.ds(0, levels - 1), pl.ds(0, down_rows), :], y_sent.at[1])
     left(full_gu.at[0], c_sent.at[0])
     left(full_down.at[:, :, :, pl.ds(0, width)], c_sent.at[1])
 
@@ -542,6 +607,16 @@
             left(full_gu.at[0, pl.ds(0, shard), :], sent.at[0, zz])
             left(full_down.at[0, zz, pl.ds(0, down_rows), :], sent.at[1, zz])
 
+        near = (zz - z == 1) | (z - zz == 1)
+
+        @pl.when(near)
+        def _():
+            left(full_down.at[0, zz, pl.ds(0, (pieces - WHOLE) * part_rows // 2), :], y_sent.at[1 + zz])
+
+        @pl.when((zz != z) & jnp.logical_not(near))
+        def _():
+            left(full_down.at[0, zz, pl.ds(0, down_rows), :], y_sent.at[1 + zz])
+
         @pl.when((zz <= z) & (z < levels - 1))
         def _():
             one(z_up)
@@ -553,6 +628,15 @@
         return 0
 
     lax.fori_loop(0, levels, drain, 0)
+
+    @pl.when(z < levels - 1)
+    def _():
+        left(full_down.at[0, z, pl.ds(0, WHOLE * part_rows // 2), :], w_sent.at[0])
+
+    @pl.when(z > 0)
+    def _():
+        left(full_down.at[0, z, pl.ds(0, WHOLE * part_rows // 2), :], w_sent.at[1])
+
     left(frecv, f_sent.at[0])
     taken(frecv, f_recv.at[0])
 
@@ -567,10 +651,21 @@
             for k in range(2)
         ]
         ffn_out = jnp.concatenate(parts, axis=1).astype(jnp.bfloat16).astype(jnp.float32)
-        out[here, :] = (after[here, :].astype(jnp.float32) + 0.5 * rms_scaled(ffn_out, gain_a[...])).astype(jnp.bfloat16)
-        return 0
+        after[here, :] = (after[here, :].astype(jnp.float32) + 0.5 * rms_scaled(ffn_out, gain_a[...])).astype(jnp.bfloat16)
+
+        @pl.when(i > 0)
+        def _():
+            written(i - 1).start()
+
+        return 0
+
+    def written(i):
+        here = pl.ds(pl.multiple_of(i * FINAL_ROWS, FINAL_ROWS), FINAL_ROWS)
+        return pltpu.make_async_copy(after.at[here, :], out.at[here, :], local_sem.at[0])
 
     lax.fori_loop(0, mine // FINAL_ROWS, finish, 0)
+    written(mine // FINAL_ROWS - 1).start()
+    pltpu.make_async_copy(after, out, local_sem.at[0]).wait()
 
 
 def fused(
@@ -591,7 +686,7 @@
         functools.partial(block_kernel, levels),
         out_shape=jax.ShapeDtypeStruct((mine, dim), bf16),
         in_specs=[whole] * 4 + [scalars] + [whole] * 2 + [vmem] * 3 + [whole] * 3,
-        out_specs=vmem,
+        out_specs=whole,
         scratch_shapes=[
             pltpu.VMEM((heads, dim), bf16),
             pltpu.VMEM((2, dim, hid), bf16),
@@ -599,7 +694,7 @@
             pltpu.VMEM(queries.shape, bf16),
             pltpu.VMEM((rows + WINDOW, key_rows.shape[1]), bf16),
             pltpu.VMEM((rows + WINDOW, value_rows.shape[1]), bf16),
-            pltpu.VMEM((1, rows + WINDOW), jnp.int32),
+            pltpu.VMEM((rows + WINDOW,), jnp.int32),
             pltpu.VMEM(queries.shape, bf16),
             pltpu.VMEM((mine, dim), bf16),
             pltpu.VMEM((rows, dim), bf16),
@@ -616,7 +711,9 @@
             dma((pieces, levels)),
             dma((2, levels)),
             dma((2, levels)),
+            dma((WHOLE, 2)),
             dma((2,)),
+            dma((1 + levels,)),
             dma((pieces, levels)),
             dma((2,)),
             dma((2 * QUARTERS + 2 * levels,)),
@@ -627,7 +724,7 @@
         ],
         compiler_params=pltpu.CompilerParams(collective_id=0, has_side_effects=True, vmem_limit_bytes=67043328),
     )(
-        queries, key_rows, value_rows, doc_ids[None], sink_logits, out_weight,
+        queries, key_rows, value_rows, doc_ids, sink_logits, out_weight,
         residual, gain_mixed[None], gain_before[None], gain_after[None], gate_weight, up_weight, down_weight,
     )
 

time: 197 us -> 191 us (0.970)
  Pallas kernels: 191 us -> 188 us
    pallas_call x1, Pallas kernels: 191 us -> 188 us  [fused(): pl.pallas_call(functools.partial(block_kernel, levels), out_shape=jax.Sha...]
where the time goes in v3:
time: 191 us
  Pallas kernels  188 us (98%)
  local copies, waits for them, and re-layouts  2.73 us (1%)
    pallas_call x1, Pallas kernels, fused(): pl.pallas_call(functools.partial(block_kernel, levels), out_shape=jax.Sha...  188 us

profile of v3, /device:TPU:0, one launch (start us, length us, event | category | flops | bytes accessed | tf_op | source)
XLA Modules:
  0.0 190.8 jit_solution(8372117612946793134)
XLA Ops:
  0.0 188.1 %shard_map.127 = bf16[384,2048]{1,0:T(8,128)(2,1)} custom-call(bf16[768,512]{1,0:T(8,128)(2,1)} %queries.1, bf16[768,256]{1,0:T(8,128)(2,1)} %keys.1, bf16[768,256]{1,0:T(8,128)(2,1)} %values.1, s32[768]{0:T(1024)} %docs.1, f32[8]{0:T(128)} %sinks.1, bf16[512,256]{1,0:T(8,128)(2,1)} %wout.1, bf16[384,2048]{1,0:T(8,128)(2,1)} %resid.1, f32[1,2048]{1,0:T(1,128)} %bitcast.3, ...), custom_call_target="tpu_custom_call" | custom-call | tf_op jit(solution)/shard_map/pallas_call | solution.py:685
  188.1 2.7 %copy.15 = bf16[384,2048]{1,0:T(8,128)(2,1)} copy(bf16[384,2048]{1,0:T(8,128)(2,1)} %shard_map.127) | data formatting | bytes 3145728

commit v4 on v3

--- a/solution.py
+++ b/solution.py
@@ -79,13 +79,15 @@
 
 MESH = pl.DeviceIdType.MESH
 QUARTERS = 4
+HALVES = 2
 SPLIT = 4
-LAG = 2
+LAG = 6
 TILE = 256
 STEP_ROWS = 32
 FINAL_ROWS = 64
 WHOLE = 1
-NORMS_AT = 11
+COPY_PARTS = 6
+NORMS_AT = 22
 
 
 def block_kernel(
@@ -112,7 +114,9 @@
     width = down.shape[1] // 2
     quarter = hid // QUARTERS
     part_rows = down_rows // SPLIT
-    chunks, pieces = 2 * QUARTERS, 2 * SPLIT
+    kinds = 2 * QUARTERS
+    chunks, pieces = kinds * HALVES, 2 * SPLIT
+    chunk_rows = half_rows // HALVES
     own_rows, peer_rows = pl.ds(pl.multiple_of(x * mine, mine), mine), pl.ds(pl.multiple_of((1 - x) * mine, mine), mine)
 
     barrier = pltpu.get_barrier_semaphore()
@@ -210,9 +214,10 @@
     def place(n, zz, cc, hh):
         stage, p = n
         if stage == 0:
-            row = pl.multiple_of(((zz * 2 + cc) * 2 + hh) * half_rows, half_rows)
-            column = pl.multiple_of((p // 2) * quarter, quarter)
-            return full_gu.at[p % 2, pl.ds(row, half_rows), pl.ds(column, quarter)]
+            kind = p // HALVES
+            row = pl.multiple_of(((zz * 2 + cc) * 2 + hh) * half_rows + p % HALVES * chunk_rows, chunk_rows)
+            column = pl.multiple_of((kind // 2) * quarter, quarter)
+            return full_gu.at[kind % 2, pl.ds(row, chunk_rows), pl.ds(column, quarter)]
         row = pl.multiple_of(hh * down_rows + (p % SPLIT) * part_rows, part_rows)
         return full_down.at[p // SPLIT, zz, pl.ds(row, part_rows), pl.ds(pl.multiple_of(cc * width, width), width)]
 
@@ -225,11 +230,11 @@
 
     def downward(n, zz):
         block = place(n, zz, c, y)
-        return remote(block, block, z_dn.at[n[0], zz], z_recv.at[at(n), zz], below)
+        return remote(block, block, z_dn.at[n[0], zz], z_recv.at[at(n), zz - 1], below)
 
     def across(n, zz, hh):
         block = place(n, zz, c, hh)
-        return remote(block, block, y_sent.at[0 if n[0] == 0 else 1 + zz], y_recv.at[at(n), zz], y_peer)
+        return remote(block, block, y_sent.at[0 if n[0] == 0 else 1 + zz], y_recv.at[at(n), jnp.where(zz > z, zz - 1, zz)], y_peer)
 
     def whole(p, side, source, device):
         block = place((1, p), source, c, 1 - y)
@@ -240,7 +245,7 @@
 
     def beside(n, zz, hh, cc):
         block = place(n, zz, cc, hh)
-        group = n[1] if n[0] == 0 else chunks + n[1] // SPLIT * levels + zz
+        group = n[1] // HALVES if n[0] == 0 else kinds + n[1] // SPLIT * levels + zz
         return remote(block, block, c_sent.at[n[0]], c_recv.at[group], c_peer)
 
     def own(stage, amount):
@@ -427,8 +432,9 @@
         columns = pl.ds(pl.multiple_of((g // 2) * quarter, quarter), quarter)
         taken(full_gu.at[g % 2, pl.ds(0, dim // 2), columns], c_recv.at[g])
 
-    def tiles_by(g):
-        return jnp.maximum(per_quarter * (g // 2) - jnp.where(g % 2 == 0, per_quarter // 2, 0), 0)
+    def tiles_at(f):
+        most = jnp.minimum(f - 2 * HALVES - 1, per_quarter * (((f + 1) // HALVES - 1) // 2))
+        return jnp.where(f < 2 * HALVES + 2, 0, most)
 
     def sent_sum(n):
         return remote(fsum.at[n, peer_rows, :], frecv.at[n], f_sent.at[0], f_recv.at[0], x_peer)
@@ -436,7 +442,7 @@
     def lowered(k, zz):
         n = k * levels + zz
         block = full_down.at[k, zz]
-        taken(block.at[:, pl.ds(pl.multiple_of((1 - c) * width, width), width)], c_recv.at[chunks + n])
+        taken(block.at[:, pl.ds(pl.multiple_of((1 - c) * width, width), width)], c_recv.at[kinds + n])
         fsum[n] = jnp.dot(hidden[...], block[...], preferred_element_type=jnp.float32).astype(jnp.bfloat16)
         sent_sum(n).start()
 
@@ -508,19 +514,21 @@
         lax.fori_loop(blocks * n // (levels + 2), blocks * (n + 1) // (levels + 2), attention, 0)
 
     lax.fori_loop(0, 3, lambda n, _: (attended(n), 0)[1], 0)
-    lax.fori_loop(1, levels, out_steps, 0)
+    lax.fori_loop(1, 2, out_steps, 0)
     steps(0, 1)
+    lax.fori_loop(2, levels, out_steps, 0)
+    steps(1, 4)
 
     def out_crossed(zz):
         out_across(zz, 1 - y).wait_recv()
         out_beside(zz, 1 - y, c).start()
 
     others(out_crossed)
-    steps(1, 2)
+    steps(4, 6)
     taken(full_out.at[:, pl.ds(0, dim // 2)], oc_recv.at[0])
     project()
     sent_projection().start()
-    steps(2, NORMS_AT)
+    steps(6, NORMS_AT)
     loads[9].wait()
     sent_projection().wait()
     norms()
@@ -530,40 +538,45 @@
     loads[7].wait()
     loads[8].wait()
     own(1, pieces)
-    steps(second, second + LAG + 2)
-    sent_normed(own_rows).wait_send()
-    sent_normed(peer_rows).wait_recv()
+    steps(second, second + LAG + 2 * HALVES)
     filled(0)
-    ratio = half_rows * quarter // (part_rows * width)
-    behind_by = LAG * ratio
-
-    def gated(g, _):
-        @pl.when(g + LAG < chunks)
-        def _():
-            line_step(0, second + g + LAG)
-
-        @pl.when(g + LAG >= chunks)
-        def _():
-            for r in range(ratio):
-                line_step(1, (g + LAG - chunks) * ratio + r)
-
-        from_side(0, second + g)
-        filled(g - 1)
-        lax.fori_loop(jnp.where(g == 2, 0, tiles_by(g - 1)), tiles_by(g), hidden_tile, 0)
-        return 0
-
-    lax.fori_loop(2, chunks, gated, 0)
-    ready = tiles_by(chunks - 1)
+    def gated(f, _):
+        g = f // HALVES
+
+        @pl.when(f + LAG < chunks)
+        def _():
+            line_step(0, second + f + LAG)
+
+        @pl.when(f + LAG >= chunks)
+        def _():
+            line_step(1, f + LAG - chunks)
+
+        from_side(0, second + f)
+
+        @pl.when(f % HALVES == HALVES - 1)
+        def _():
+            filled(g - 1)
+
+        @pl.when(f == 2 * HALVES + 2)
+        def _():
+            sent_normed(own_rows).wait_send()
+            sent_normed(peer_rows).wait_recv()
+
+        lax.fori_loop(tiles_at(f - 1), tiles_at(f), hidden_tile, 0)
+        return 0
+
+    lax.fori_loop(2 * HALVES, chunks, gated, 0)
+    ready = tiles_at(chunks - 1)
     rest = hid // TILE - ready
 
     def lowering(u, _):
         line_step(1, u)
-        v = u - behind_by
+        v = u - LAG
         from_side(1, v)
 
         @pl.when(v == 0)
         def _():
-            filled(chunks - 1)
+            filled(kinds - 1)
 
         lax.fori_loop(jnp.minimum(ready + v, hid // TILE), jnp.minimum(ready + v + 1, hid // TILE), hidden_tile, 0)
 
@@ -577,14 +590,14 @@
 
         return 0
 
-    lax.fori_loop(behind_by, lowers, lowering, 0)
+    lax.fori_loop(LAG, lowers, lowering, 0)
 
     def ending(v, _):
         from_side(1, v)
         settled(v - 1)
         return 0
 
-    lax.fori_loop(lowers - behind_by, lowers, ending, 0)
+    lax.fori_loop(lowers - LAG, lowers, ending, 0)
     settled(jnp.int32(lowers - 1))
 
     @pl.when(s < count - 1)
@@ -666,6 +679,40 @@
     lax.fori_loop(0, mine // FINAL_ROWS, finish, 0)
     written(mine // FINAL_ROWS - 1).start()
     pltpu.make_async_copy(after, out, local_sem.at[0]).wait()
+
+
+def copy_kernel(source, target, held, arrived, left):
+    parts = held.shape[0]
+    rows = held.shape[1]
+
+    def taken(n):
+        return pltpu.make_async_copy(source.at[pl.ds(n * rows, rows), :], held.at[n], arrived.at[n])
+
+    def given(n):
+        return pltpu.make_async_copy(held.at[n], target.at[pl.ds(n * rows, rows), :], left.at[n])
+
+    for n in range(parts):
+        taken(n).start()
+    for n in range(parts):
+        taken(n).wait()
+        given(n).start()
+    for n in range(parts):
+        given(n).wait()
+
+
+def copied(array):
+    parts, whole = COPY_PARTS, pl.BlockSpec(memory_space=pl.ANY)
+    return pl.pallas_call(
+        copy_kernel,
+        out_shape=jax.ShapeDtypeStruct(array.shape, array.dtype),
+        in_specs=[whole],
+        out_specs=whole,
+        scratch_shapes=[
+            pltpu.VMEM((parts, array.shape[0] // parts, array.shape[1]), array.dtype),
+            pltpu.SemaphoreType.DMA((parts,)),
+            pltpu.SemaphoreType.DMA((parts,)),
+        ],
+    )(array)
 
 
 def fused(
@@ -681,7 +728,7 @@
     vmem, whole = pl.BlockSpec(memory_space=pltpu.VMEM), pl.BlockSpec(memory_space=pl.ANY)
     scalars = pl.BlockSpec(memory_space=pltpu.SMEM)
     bf16, dma = jnp.bfloat16, pltpu.SemaphoreType.DMA
-    pieces = 2 * QUARTERS + 2 * SPLIT
+    pieces = 2 * QUARTERS * HALVES + 2 * SPLIT
     return pl.pallas_call(
         functools.partial(block_kernel, levels),
         out_shape=jax.ShapeDtypeStruct((mine, dim), bf16),
@@ -708,13 +755,13 @@
             dma((levels,)),
             dma((levels,)),
             dma((1,)),
-            dma((pieces, levels)),
+            dma((pieces, levels - 1)),
             dma((2, levels)),
             dma((2, levels)),
             dma((WHOLE, 2)),
             dma((2,)),
             dma((1 + levels,)),
-            dma((pieces, levels)),
+            dma((pieces, levels - 1)),
             dma((2,)),
             dma((2 * QUARTERS + 2 * levels,)),
             dma((2,)),
@@ -746,9 +793,11 @@
 ):
     pairs = lax.axis_size("grp") == 2 and lax.axis_size("tp") == 2
     if pairs and lax.axis_size("sp") % 2 == 0 and lax.axis_size("sp") >= 8:
-        return fused(
-            queries, key_rows, value_rows, doc_ids, sink_logits, out_weight,
-            residual, gain_mixed, gain_before, gain_after, gate_weight, up_weight, down_weight,
+        return copied(
+            fused(
+                queries, key_rows, value_rows, doc_ids, sink_logits, out_weight,
+                residual, gain_mixed, gain_before, gain_after, gate_weight, up_weight, down_weight,
+            )
         )
     mixed = attend(queries, key_rows, value_rows, doc_ids, sink_logits)
     head_columns = lax.all_gather(out_weight, "sp", axis=1, tiled=True)

time: 191 us -> 190 us (level)
  local copies, waits for them, and re-layouts: 2.73 us -> 0 us
  Pallas kernels: 188 us -> 190 us
    unnamed x1 -> x0, local copies, waits for them, and re-layouts: 2.73 us -> none
    pallas_call x0 -> x1, Pallas kernels: none -> 2.19 us  [copied(): pl.pallas_call(copy_kernel, out_shape=jax.ShapeDtypeStruct(array.shape, a...]
where the time goes in v4:
time: 190 us
  Pallas kernels  190 us (100%)
    pallas_call x1, Pallas kernels, fused(): pl.pallas_call(functools.partial(block_kernel, levels), out_shape=jax.Sha...  188 us

profile of v4, /device:TPU:0, one launch (start us, length us, event | category | flops | bytes accessed | tf_op | source)
XLA Modules:
  0.0 190.1 jit_solution(10496305742128916005)
XLA Ops:
  0.0 187.9 %shard_map.127.source = bf16[384,2048]{1,0:T(8,128)(2,1)} custom-call(bf16[768,512]{1,0:T(8,128)(2,1)} %queries.1, bf16[768,256]{1,0:T(8,128)(2,1)} %keys.1, bf16[768,256]{1,0:T(8,128)(2,1)} %values.1, s32[768]{0:T(1024)} %docs.1, f32[8]{0:T(128)} %sinks.1, bf16[512,256]{1,0:T(8,128)(2,1)} %wout.1, bf16[384,2048]{1,0:T(8,128)(2,1)} %resid.1, ...), custom_call_target="tpu_custom_call" | custom-call | tf_op jit(solution)/shard_map/pallas_call | solution.py:732
  187.9 2.2 %shard_map.128 = bf16[384,2048]{1,0:T(8,128)(2,1)} custom-call(bf16[384,2048]{1,0:T(8,128)(2,1)} %shard_map.127.source), custom_call_target="tpu_custom_call" | custom-call | tf_op jit(solution)/shard_map/pallas_call | solution.py:705
